TPU v7x, 256 devices: a whole 4x4x8 slice. The times are simulated.
256 devices in a mesh: st: 32 (over z, x), tp: 8 (over y, core).
Axes of the slice: x: 4, y: 4, z: 8, core: 2. Of those that a mesh axis runs over, the one named last changes fastest.
Arguments:
- tokens: bfloat16 [16384, 2048], P('st'), may hold values from -6 to 6
- mix_query: bfloat16 [2048, 1024], P(None, 'tp'), may hold values from -0.125 to 0.125
- mix_key: bfloat16 [2048, 1024], P(None, 'tp'), may hold values from -0.125 to 0.125
- mix_value: bfloat16 [2048, 1024], P(None, 'tp'), may hold values from -0.125 to 0.125
- decay_lower_map: bfloat16 [2048, 64], replicated, may hold values from -0.125 to 0.125
- decay_upper_map: bfloat16 [64, 1024], P(None, 'tp'), may hold values from -1 to 1
- decay_base: float32 [1024], P('tp'), may hold values from -7.5 to -2.5
- decay_shift: float32 [16384, 16], P('st', 'tp'), may hold values from -3.8 to 9.8
- rate_lower_map: bfloat16 [2048, 64], replicated, may hold values from -0.125 to 0.125
- rate_upper_map: bfloat16 [64, 1024], P(None, 'tp'), may hold values from -0.75 to 0.75
- norm_gain: float32 [1024], P('tp'), may hold values from 0.1 to 1.9
- mix_out: bfloat16 [1024, 2048], P(None, 'tp'), may hold values from -0.1875 to 0.1875
- cross_query: bfloat16 [2048, 2048], P(None, 'tp'), may hold values from -0.125 to 0.125
- score_gain: float32 [2048], P('tp'), may hold values from 0.1 to 1.9
- passage_key: bfloat16 [2048, 2048], P(None, 'tp'), may hold values from -0.125 to 0.125
- passage_value: bfloat16 [2048, 2048], P(None, 'tp'), may hold values from -0.125 to 0.125
- cross_out: bfloat16 [2048, 2048], P(None, 'tp'), may hold values from -0.5 to 0.5
- gate_down: bfloat16 [2048, 128], replicated, may hold values from -0.125 to 0.125
- gate_up: bfloat16 [128, 2048], P(None, 'tp'), may hold values from -0.5 to 0.5
- store: bfloat16 [384, 96, 2048], P('st'), may hold values from -6 to 6
- passage_ids: int32 [256, 4], P('st'), may hold values from 0 to 383, as said below
Outputs:
- mixed: bfloat16 [16384, 2048], P('st', 'tp')
Inputs may be any that keep to these rules, and one draw needn't show every extreme that they name: `passage_ids`: among the 32 passages named by the rows of one sequence, at most 2 are held by one index of st (passage p by index p // 12); in every draw exactly 2 are held by the index before the sequence's own.
All inputs are finite; a program needn't handle non-finite values.
Results may differ from a plain program's by a relative error of at most 0.0075.
Values may be sent and summed in bfloat16 or wider, within the bound.
A program may use at most 128 MiB of HBM per device.

v0:
```python
import jax
import jax.numpy as jnp
from jax import lax
from jax.sharding import PartitionSpec as P

XHEAD = 256
QBLOCK = 64
MBLOCK = 64


FLOAT32 = jnp.float32
BFLOAT = jnp.bfloat16
PRECISE = lax.Precision.HIGHEST


def in_one_piece(arrays, axis, dim, along):
    ends, at = ([], 0)
    for a in arrays[:-1]:
        at += a.shape[along]
        ends.append(at)
    both = jnp.concatenate(arrays, axis=along)
    return tuple(jnp.split(lax.all_gather(both, axis, axis=dim, tiled=True), ends, axis=along))


def rounded(values):
    return lax.optimization_barrier(values.astype(BFLOAT)).astype(FLOAT32)


def head_norm(values, head_size):
    shaped = values.reshape(values.shape[:-1] + (values.shape[-1] // head_size, head_size))
    scaled = shaped * lax.rsqrt(jnp.mean(shaped * shaped, axis=-1, keepdims=True) + 1e-06)
    return scaled.reshape(values.shape)


def pair_dots(left, right):
    return jnp.einsum("hsc,htc->hst", left, right, precision=PRECISE)


def apply_mat(matrix, vectors):
    return jnp.einsum("hst,htc->hsc", matrix, vectors, precision=PRECISE)


def block_step(state, inputs):
    query_vec, key_vec, value_vec, minus_key, rate_key, log_fade = inputs
    length = query_vec.shape[1]
    cumul_log = jnp.cumsum(log_fade, axis=1)
    before = cumul_log - log_fade
    block_end = cumul_log[:, -1:, :]
    row_idx = lax.broadcasted_iota(jnp.int32, (length, length), 0)
    col_idx = lax.broadcasted_iota(jnp.int32, (length, length), 1)
    strict = (col_idx < row_idx).astype(FLOAT32)
    upto_mask = (col_idx <= row_idx).astype(FLOAT32)
    minus_scaled = minus_key * jnp.exp(before)
    query_scaled = query_vec * jnp.exp(cumul_log)
    key_inverse = key_vec * jnp.exp(-cumul_log)
    rate_inverse = rate_key * jnp.exp(-cumul_log)
    key_pull = pair_dots(minus_scaled, key_inverse) * strict
    rate_pull = pair_dots(minus_scaled, rate_inverse) * strict
    key_read = pair_dots(query_scaled, key_inverse) * upto_mask
    rate_read = pair_dots(query_scaled, rate_inverse) * upto_mask
    solved = jnp.einsum("hsj,hij->hsi", minus_scaled, state, precision=PRECISE) + apply_mat(
        key_pull, value_vec
    )
    power_mat = rate_pull
    for repeat_idx in range((length - 1).bit_length()):
        solved = solved + apply_mat(power_mat, solved)
        power_mat = jnp.einsum("hst,htu->hsu", power_mat, power_mat, precision=PRECISE)
    outputs = (
        jnp.einsum("hsj,hij->hsi", query_scaled, state, precision=PRECISE)
        + apply_mat(key_read, value_vec)
        + apply_mat(rate_read, solved)
    )
    fade_out = jnp.exp(block_end - cumul_log)
    state = (
        state * jnp.exp(block_end)
        + jnp.einsum("hsi,hsj->hij", value_vec, key_vec * fade_out, precision=PRECISE)
        + jnp.einsum("hsi,hsj->hij", solved, rate_key * fade_out, precision=PRECISE)
    )
    return (state, outputs)


def mixer(
    tokens,
    mix_query,
    mix_key,
    mix_value,
    decay_lower_map,
    decay_upper_map,
    decay_base,
    decay_shift,
    rate_lower_map,
    rate_upper_map,
    norm_gain,
):
    tok_rows = tokens.shape[0]
    head_count = decay_shift.shape[1]
    mix_width = mix_query.shape[1]
    head_size = mix_width // head_count

    def project(weight):
        return rounded(jnp.dot(tokens, weight, preferred_element_type=FLOAT32))

    query_vec = project(mix_query)
    key_vec = project(mix_key)
    value_vec = project(mix_value)
    decay_low = jnp.tanh(jnp.dot(tokens, decay_lower_map, preferred_element_type=FLOAT32)).astype(
        BFLOAT
    )
    decay_pre = (
        decay_base
        + jnp.dot(decay_low, decay_upper_map, preferred_element_type=FLOAT32)
        + jnp.repeat(decay_shift, head_size, axis=1)
    )
    log_fade = -jnp.exp(-jax.nn.softplus(-decay_pre) - 0.5)
    rate_low = jnp.dot(tokens, rate_lower_map, preferred_element_type=FLOAT32).astype(BFLOAT)
    rate_gate = jax.nn.sigmoid(jnp.dot(rate_low, rate_upper_map, preferred_element_type=FLOAT32))

    def to_blocks(values):
        shaped = values.reshape(tok_rows // MBLOCK, MBLOCK, head_count, head_size)
        return shaped.transpose(0, 2, 1, 3)

    keyed = key_vec.reshape(tok_rows, head_count, head_size)
    unit_key = keyed * lax.rsqrt(jnp.sum(keyed * keyed, axis=-1, keepdims=True) + 1e-06)
    rate_key = unit_key * rate_gate.reshape(tok_rows, head_count, head_size)
    block_in = (
        to_blocks(query_vec),
        to_blocks(key_vec),
        to_blocks(value_vec),
        to_blocks(-unit_key),
        to_blocks(rate_key),
        to_blocks(log_fade),
    )
    state_zero = jnp.zeros((head_count, head_size, head_size), FLOAT32)
    _, head_out = lax.scan(block_step, state_zero, block_in)
    head_out = head_out.transpose(0, 2, 1, 3).reshape(tok_rows, head_count, head_size)
    centred = head_out - jnp.mean(head_out, axis=-1, keepdims=True)
    spread = jnp.mean(centred * centred, axis=-1, keepdims=True)
    normed = (centred * lax.rsqrt(spread + 0.00064)).reshape(tok_rows, mix_width)
    return (normed * norm_gain).astype(BFLOAT)


def local(
    tokens,
    mix_query,
    mix_key,
    mix_value,
    decay_lower_map,
    decay_upper_map,
    decay_base,
    decay_shift,
    rate_lower_map,
    rate_upper_map,
    norm_gain,
    mix_out,
    cross_query,
    score_gain,
    passage_key,
    passage_value,
    cross_out,
    gate_down,
    gate_up,
    store,
    passage_ids,
):
    mixer_heads = mixer(
        tokens,
        mix_query,
        mix_key,
        mix_value,
        decay_lower_map,
        decay_upper_map,
        decay_base,
        decay_shift,
        rate_lower_map,
        rate_upper_map,
        norm_gain,
    )
    tok_rows = tokens.shape[0]
    model_width = tokens.shape[1]
    owner_count = lax.axis_size("st")
    pass_dev = store.shape[0]
    passage_len = store.shape[1]
    cross_width = cross_query.shape[1]
    head_count = cross_width // XHEAD
    flat_ids = passage_ids.reshape(-1)
    slot_count = flat_ids.shape[0]
    capacity = max(2, -(-slot_count // owner_count))
    owner_of = flat_ids // pass_dev
    local_idx = flat_ids % pass_dev
    slot_order = jnp.arange(slot_count)
    earlier_same = (owner_of[:, None] == owner_of[None, :]) & (
        slot_order[None, :] < slot_order[:, None]
    )
    slot_rank = jnp.sum(earlier_same.astype(jnp.int32), axis=1)
    to_owner = owner_of[:, None] == jnp.arange(owner_count)[None, :]
    to_slot = slot_rank[:, None] == jnp.arange(capacity)[None, :]
    wanted = jnp.sum(
        jnp.where(to_owner[:, :, None] & to_slot[:, None, :], local_idx[:, None, None] + 1, 0),
        axis=0,
    )
    asked = lax.all_to_all(wanted, "st", split_axis=0, concat_axis=0, tiled=True)
    served = jnp.maximum(asked.reshape(-1) - 1, 0)
    where_from = owner_of * capacity + slot_rank
    row_share = passage_len // lax.axis_size("tp")
    own_rows = lax.dynamic_slice_in_dim(store, lax.axis_index("tp") * row_share, row_share, 1)
    outgoing = own_rows[served].reshape(owner_count, capacity, row_share, model_width)
    incoming = lax.all_to_all(outgoing, "st", split_axis=0, concat_axis=0, tiled=True)
    picked = incoming.reshape(owner_count * capacity, row_share, model_width)[where_from]
    piece = lax.all_gather(picked, "tp", axis=1, tiled=True)
    flat_rows = piece.reshape(-1, model_width)
    keyed = head_norm(
        jnp.dot(flat_rows, passage_key, preferred_element_type=FLOAT32), XHEAD
    ).astype(BFLOAT)
    valued = jnp.dot(flat_rows, passage_value, preferred_element_type=FLOAT32).astype(BFLOAT)
    joined = jnp.concatenate([keyed, valued], axis=-1)
    projected = joined.reshape(piece.shape[0], piece.shape[1], 2 * cross_width)
    block_count = tok_rows // QBLOCK
    queries = (
        head_norm(jnp.dot(tokens, cross_query, preferred_element_type=FLOAT32), XHEAD) * score_gain
    )
    queries = queries.astype(BFLOAT).reshape(block_count, QBLOCK, head_count, XHEAD)
    block_keys = projected[:, :, :cross_width].reshape(block_count, -1, head_count, XHEAD)
    block_values = projected[:, :, cross_width:].reshape(block_count, -1, head_count, XHEAD)
    scores = jnp.einsum(
        "bqhd,bkhd->bhqk", queries, block_keys, preferred_element_type=FLOAT32
    ) * XHEAD ** (-0.5)
    expon = jnp.exp(scores)
    weights = (expon / jnp.sum(expon, axis=-1, keepdims=True)).astype(BFLOAT)
    attended = jnp.einsum("bhqk,bkhd->bqhd", weights, block_values, preferred_element_type=FLOAT32)
    attended = attended.astype(BFLOAT).reshape(tok_rows, cross_width)
    shard_total = lax.axis_size("tp")
    out_cols = mix_out.shape[1]
    mix_rows = mix_out.reshape(shard_total, -1, out_cols)
    cross_rows = cross_out.reshape(shard_total, -1, out_cols)
    pieces = in_one_piece((mixer_heads[None], attended[None]), "tp", 0, 2)
    mixer_part = jnp.einsum("ntc,ncd->td", pieces[0], mix_rows, preferred_element_type=FLOAT32)
    cross_part = jnp.einsum("ntc,ncd->td", pieces[1], cross_rows, preferred_element_type=FLOAT32)
    gate_low = jnp.dot(tokens, gate_down, preferred_element_type=FLOAT32).astype(BFLOAT)
    gate_open = jax.nn.sigmoid(jnp.dot(gate_low, gate_up, preferred_element_type=FLOAT32))
    return (mixer_part + gate_open * cross_part).astype(BFLOAT)


def solution(mesh):
    placed = (
        P("st", None),
        P(None, "tp"),
        P(None, "tp"),
        P(None, "tp"),
        P(),
        P(None, "tp"),
        P("tp"),
        P("st", "tp"),
        P(),
        P(None, "tp"),
        P("tp"),
        P(None, "tp"),
        P(None, "tp"),
        P("tp"),
        P(None, "tp"),
        P(None, "tp"),
        P(None, "tp"),
        P(),
        P(None, "tp"),
        P("st", None, None),
        P("st", None),
    )
    return jax.shard_map(
        local, mesh=mesh, in_specs=placed, out_specs=P("st", "tp"), check_vma=False
    )
```

profile of v0, /device:TPU:1, one launch (start us, length us, event | category | flops | bytes accessed | tf_op | source)
XLA Modules:
  0.0 331.7 jit_solution(13598278749513852228)
XLA Ops:
  9.7 11.9 %all-to-all-start = ((s32[32,1,2]{2,1,0:T(1,128)}), s32[32,1,2]{2,1,0:T(1,128)S(1)}, u32[]{:S(2)}, u32[]{:S(2)}) async-start(s32[32,1,2]{2,1,0:T(1,128)} %copy.164), calls=%async_computation | async-start | bytes 32768 | tf_op jit(solution)/shard_map/all_to_all | solution.py:201
  21.5 1.5 constant_dynamic-slice_fusion
  23.1 7.0 %all-to-all-done = s32[32,1,2]{2,1,0:T(1,128)S(1)} async-done(((s32[32,1,2]{2,1,0:T(1,128)}), s32[32,1,2]{2,1,0:T(1,128)S(1)}, u32[]{:S(2)}, u32[]{:S(2)}) %all-to-all-start) | async-done | bytes 288 | tf_op jit(solution)/shard_map/all_to_all | solution.py:201
  30.2 2.7 gather_fusion
  33.0 7.2 %copy.166 = bf16[32,2,12,2048]{3,1,2,0:T(2,128)(2,1)} copy(bf16[32,2,12,2048]{3,2,1,0:T(8,128)(2,1)} %bitcast.256) | data formatting | bytes 6291456 | tf_op jit(solution)/shard_map/reshape | solution.py:206
  40.2 4.9 %all-to-all-start.1 = ((bf16[32,2,12,2048]{3,1,2,0:T(2,128)(2,1)}), bf16[32,2,12,2048]{3,1,2,0:T(2,128)(2,1)}, u32[]{:S(2)}, u32[]{:S(2)}) async-start(bf16[32,2,12,2048]{3,1,2,0:T(2,128)(2,1)} %copy.166), calls=%async_computation.1 | async-start | bytes 6291456 | tf_op jit(solution)/shard_map/all_to_all | solution.py:207
  47.8 2.7 fusion.48
  50.5 2.1 reshape.421
  54.6 2.1 fusion.57
  59.0 1.7 convolution_convert_fusion.5
  61.8 2.0 copy.150
  63.9 2.9 fusion.51
  66.8 48.7 %all-to-all-done.1 = bf16[32,2,12,2048]{3,1,2,0:T(2,128)(2,1)} async-done(((bf16[32,2,12,2048]{3,1,2,0:T(2,128)(2,1)}), bf16[32,2,12,2048]{3,1,2,0:T(2,128)(2,1)}, u32[]{:S(2)}, u32[]{:S(2)}) %all-to-all-start.1) | async-done | bytes 3145760 | tf_op jit(solution)/shard_map/all_to_all | solution.py:207
  115.5 5.4 %copy.180 = bf16[32,2,12,2048]{3,2,1,0:T(8,128)(2,1)} copy(bf16[32,2,12,2048]{3,1,2,0:T(2,128)(2,1)} %all-to-all-done.1) | data formatting | bytes 6291456 | tf_op jit(solution)/shard_map/reshape | solution.py:208
  120.9 4.2 %gather_fusion.1 = bf16[32,12,2048]{2,1,0:T(8,128)(2,1)} fusion(bf16[64,12,2048]{2,1,0:T(8,128)(2,1)} %bitcast.260, s32[1024]{0:T(1024)S(1)} %pad_clamp_fusion), kind=kCustom, calls=%fused_computation.1 | custom fusion | bytes 3145856 | tf_op jit(solution)/shard_map/gather | solution.py:208
  125.1 3.7 %copy.171 = bf16[32,12,2048]{2,0,1:T(8,128)(2,1)} copy(bf16[32,12,2048]{2,1,0:T(8,128)(2,1)} %gather_fusion.1) | data formatting | bytes 3145728 | tf_op jit(solution)/shard_map/gather | solution.py:208
  129.1 109.5 %while.13 = (s32[]{:T(128)}, f32[2,64,64]{2,1,0:T(8,128)S(1)}, f32[8,2,64,64]{3,2,1,0:T(8,128)S(1)}, f32[8,2,64,64]{3,2,1,0:T(8,128)S(1)}, f32[8,2,64,64]{2,3,1,...) while((s32[]{:T(128)}, f32[2,64,64]{2,1,0:T(8,128)S(1)}, ...), condition=%wide.region_3.4_spmd.clone, body=%wide.region_1.3_spmd.clone.sunk | while | flops 139272192 | bytes 4008589 | solution.py:134
  141.6 1.2 convolution_add_fusion.30
  144.0 1.2 convolution_multiply_fusion.9
  155.4 1.2 convolution_add_fusion.30
  240.0 2.0 multiply_reduce_fusion.1
  242.2 14.6 %copy.172 = bf16[32,96,2048]{2,1,0:T(8,128)(2,1)} copy(bf16[32,96,2048]{2,0,1:T(8,128)(2,1)} %all-gather.6.cloned.1.call-done) | data formatting | bytes 25165824 | tf_op jit(solution)/shard_map/all_gather | solution.py:209
  256.9 6.9 %multiply_reduce_fusion = (f32[3072]{0:T(1024)S(1)}, f32[3072,256]{0,1:T(8,128)S(1)}) fusion(bf16[3072,2048]{1,0:T(8,128)(2,1)} %bitcast.257, bf16[2048,256]{1,0:T(8,128)(2,1)S(1)} %copy-done.6), kind=kOutput, calls=%fused_computation.64 | convolution fusion | flops 3222795264 | bytes 16789504 | tf_op jit(solution)/shard_map/dot_general | solution.py:212
  263.8 8.1 %convolution_convert_fusion = bf16[3072,256]{0,1:T(8,128)(2,1)S(1)} fusion(bf16[3072,2048]{1,0:T(8,128)(2,1)} %bitcast.258, bf16[2048,256]{1,0:T(8,128)(2,1)S(1)} %copy-done.7), kind=kOutput, calls=%fused_computation.61 | convolution fusion | flops 3222011904 | bytes 15204352 | tf_op jit(solution)/shard_map/dot_general | solution.py:214
  272.1 1.9 pad_maximum_fusion
  274.0 4.7 %copy.173 = bf16[3072,512]{1,0:T(8,128)(2,1)} copy(bf16[3072,512]{0,1:T(8,128)(2,1)} %pad_maximum_fusion) | data formatting | bytes 6291456 | tf_op jit(solution)/shard_map/concatenate | solution.py:215
  278.7 3.2 fusion.69
  282.6 1.9 convolution_convert_fusion.1
  285.3 30.9 %all-gather.4.cloned.1.call-done = bf16[8,512,384]{2,1,0:T(8,128)(2,1)} async-done(((bf16[1,512,384]{2,1,0:T(8,128)(2,1)}), bf16[8,512,384]{2,1,0:T(8,128)(2,1)}) %all-gather.4.cloned.1.call-update) | async-done | bytes 3145744 | tf_op jit(solution)/shard_map/all_gather | solution.py:22
  316.2 2.6 convolution_bitcast_fusion
  318.8 3.1 fusion.35
  321.9 3.0 fusion.43
  (300 shorter events, 119.0 us)
Async XLA Ops:
  6.5 39.1 %copy-start = (bf16[512,2048]{1,0:T(8,128)(2,1)S(1)}, bf16[512,2048]{1,0:T(8,128)(2,1)}, u32[]{:S(2)}) copy-start(bf16[512,2048]{1,0:T(8,128)(2,1)} %param.23) | copy-start | bytes 6291460
  9.7 20.4 %all-to-all-start = ((s32[32,1,2]{2,1,0:T(1,128)}), s32[32,1,2]{2,1,0:T(1,128)S(1)}, u32[]{:S(2)}, u32[]{:S(2)}) async-start(s32[32,1,2]{2,1,0:T(1,128)} %copy.164), calls=%async_computation | async-start | bytes 32768 | tf_op jit(solution)/shard_map/all_to_all | solution.py:201
  40.2 5.5 %copy-start.1 = (bf16[2048,128]{1,0:T(8,128)(2,1)S(1)}, bf16[2048,128]{1,0:T(8,128)(2,1)}, u32[]{:S(2)}) copy-start(bf16[2048,128]{1,0:T(8,128)(2,1)} %param.25) | copy-start | bytes 1572868
  40.2 75.3 %all-to-all-start.1 = ((bf16[32,2,12,2048]{3,1,2,0:T(2,128)(2,1)}), bf16[32,2,12,2048]{3,1,2,0:T(2,128)(2,1)}, u32[]{:S(2)}, u32[]{:S(2)}) async-start(bf16[32,2,12,2048]{3,1,2,0:T(2,128)(2,1)} %copy.166), calls=%async_computation.1 | async-start | bytes 6291456 | tf_op jit(solution)/shard_map/all_to_all | solution.py:207
  45.1 197.1 %all-gather.6.cloned.1.call-start = ((), (), s32[]{:S(2)}) async-start(), calls=%async_computation.3 | async-start | bytes 14155776 | tf_op jit(solution)/shard_map/all_gather | solution.py:209
  45.6 2.2 copy-start.10
  47.7 4.9 %copy-start.2 = (bf16[2048,128]{1,0:T(8,128)(2,1)S(1)}, bf16[2048,128]{1,0:T(8,128)(2,1)}, u32[]{:S(2)}) copy-start(bf16[2048,128]{1,0:T(8,128)(2,1)} %param.24) | copy-start | bytes 1572868
  50.5 3.9 %copy-start.3 = (f32[512,2]{0,1:T(2,128)S(1)}, f32[512,2]{0,1:T(2,128)}, u32[]{:S(2)}) copy-start(f32[512,2]{0,1:T(2,128)} %param.30) | copy-start | bytes 12292
  52.6 2.0 copy-start.11
  52.6 2.0 copy-start.12
  128.8 187.4 %all-gather.4.cloned.1.call-start = ((), (), s32[]{:S(2)}) async-start(), calls=%async_computation.2 | async-start | bytes 3538944 | tf_op jit(solution)/shard_map/all_gather | solution.py:22
  238.6 1.2 copy-start.5
  242.2 14.6 %copy-start.6 = (bf16[2048,256]{1,0:T(8,128)(2,1)S(1)}, bf16[2048,256]{1,0:T(8,128)(2,1)}, u32[]{:S(2)}) copy-start(bf16[2048,256]{1,0:T(8,128)(2,1)} %param.37) | copy-start | bytes 3145732
  256.9 6.9 %copy-start.7 = (bf16[2048,256]{1,0:T(8,128)(2,1)S(1)}, bf16[2048,256]{1,0:T(8,128)(2,1)}, u32[]{:S(2)}) copy-start(bf16[2048,256]{1,0:T(8,128)(2,1)} %param.38) | copy-start | bytes 3145732
  278.7 3.3 copy-start.4
  284.4 34.3 %copy-start.8 = (bf16[2048,256]{1,0:T(8,128)(2,1)S(1)}, bf16[2048,256]{1,0:T(8,128)(2,1)}, u32[]{:S(2)}) copy-start(bf16[2048,256]{1,0:T(8,128)(2,1)} %param.39) | copy-start | bytes 3145732
  318.8 3.1 copy-start.9
Sparse Core Ops, SparseCore 0:
  128.9 70.4 all-gather.5
  285.4 30.7 all-gather.3
where the time goes:
time: 337 us; the launch traced here: 332 us
  matrix products  143 us (42%)
  waiting for transfers between devices  86.7 us (26%)
  local copies, waits for them, and re-layouts  59.7 us (18%)
  starting transfers between devices  17.3 us (5%)
  between operations  13.8 us (4%)
  other arithmetic  9.73 us (3%)
    all_to_all x1, waiting for transfers between devices, local(): lax.all_to_all(outgoing, 'st', split_axis=0, concat_axis=0, tiled=True)  48.7 us
    dot_general x32, matrix products, pair_dots(): return jnp.einsum('hsc,htc->hst', left, right, precision=PRECISE)  35.9 us
    all_gather x1, waiting for transfers between devices, in_one_piece(): lax.all_gather(both, axis, axis=dim, tiled=True)  30.9 us
    dot_general x72, matrix products, apply_mat(): return jnp.einsum('hst,htc->hsc', matrix, vectors, precision=PRECISE)  28 us
    all_gather x1, local copies, waits for them, and re-layouts, local(): piece = lax.all_gather(picked, 'tp', axis=1, tiled=True)  14.6 us
    all_to_all x1, starting transfers between devices, local(): lax.all_to_all(wanted, 'st', split_axis=0, concat_axis=0, tiled=True)  11.9 us
    dot_general x8, matrix products, block_step(): jnp.einsum('hsi,hsj->hij', solved, rate_key * fade_out, precision=PRECISE)  9.14 us
    dot_general x8, matrix products, block_step(): jnp.einsum('hsi,hsj->hij', value_vec, key_vec * fade_out, precision=PRECISE)  8.7 us
  transfers between devices with their start and end apart: 4, of which 3 were waited for; matrix products, arithmetic and copies ran while one was open for 40% of the time, Pallas kernels for 0%

commit v1 on v0

v1 whole, which is shorter than its diff:
```python
import functools
import math

import jax
import jax.numpy as jnp
from jax import lax
from jax.experimental import pallas as pl
from jax.experimental.pallas import tpu as pltpu
from jax.sharding import PartitionSpec as P

F32 = jnp.float32
BF = jnp.bfloat16
NZ, NX = 8, 4
QBLOCK = 64
VMEM = pl.BlockSpec(memory_space=pltpu.VMEM)
MESH = pl.DeviceIdType.MESH
HBM = pl.BlockSpec(memory_space=pltpu.HBM)
SMEM = pl.BlockSpec(memory_space=pltpu.SMEM)
ANY = pl.BlockSpec(memory_space=pl.ANY)


def dg(a, b, ca, cb):
    return lax.dot_general(a, b, (((ca,), (cb,)), ((), ())), preferred_element_type=F32)


def bdot(a, b, ca=1, cb=0):
    return dg(a.astype(BF), b.astype(BF), ca, cb)


def cost(flops):
    return pl.CostEstimate(flops=int(flops), bytes_accessed=int(4e6), transcendentals=0)


def params(mib, **kw):
    return pltpu.CompilerParams(vmem_limit_bytes=mib * 1024 * 1024, **kw)


def head_normed(y):
    return y * lax.rsqrt(jnp.mean(y * y, axis=-1, keepdims=True) + 1e-06)


def exact_sum_dot(left, x, ca, cb, swap):
    hi = x.astype(BF)
    r = x - hi.astype(F32)
    mid = r.astype(BF)
    low = (r - mid.astype(F32)).astype(BF)
    parts = [dg(p, left, ca, cb) if swap else dg(left, p, ca, cb) for p in (hi, mid, low)]
    return parts[0] + parts[1] + parts[2]


def mixer_stages(tok, wq, wk, wv, wdl, wdu, base, shift, wrl, wru, gain, out,
                 s_a, s_q, s_ki, s_ri, s_kf, s_rf, s_vs, s_e, s_o):
    t = tok[...]
    rows = t.shape[0]
    chunks = rows // 64
    lane = lax.broadcasted_iota(jnp.int32, (64, 128), 1)
    row = lax.broadcasted_iota(jnp.int32, (64, 128), 0)
    left = lane < 64
    in_head = jnp.where(left, lane, lane - 64)
    sl = left & (in_head < row)
    sr = jnp.logical_not(left) & (in_head < row)
    upto = in_head <= row
    r2 = lax.broadcasted_iota(jnp.int32, (128, 128), 0)
    l2 = lax.broadcasted_iota(jnp.int32, (128, 128), 1)
    same = (r2 < 64) == (l2 < 64)
    eye = r2 == l2
    ones = jnp.where(same, 1.0, 0.0).astype(BF)
    tri = jnp.where(
        lax.broadcasted_iota(jnp.int32, (64, 64), 1) <= lax.broadcasted_iota(jnp.int32, (64, 64), 0),
        1.0, 0.0).astype(BF)
    q = dg(t, wq[...], 1, 0).astype(BF).astype(F32)
    k = dg(t, wk[...], 1, 0).astype(BF).astype(F32)
    v = dg(t, wv[...], 1, 0).astype(BF).astype(F32)
    low = jnp.tanh(dg(t, wdl[...], 1, 1)).astype(BF)
    spread2 = jnp.where(
        (lax.broadcasted_iota(jnp.int32, (2, 128), 1) < 64)
        == (lax.broadcasted_iota(jnp.int32, (2, 128), 0) == 0), 1.0, 0.0).astype(BF)
    pre = base[...] + dg(low, wdu[...], 1, 0) + exact_sum_dot(spread2, shift[...], 0, 0, True)
    log_fade = jax.nn.sigmoid(pre) * (-math.exp(-0.5))
    rate_low = dg(t, wrl[...], 1, 1).astype(BF)
    rate = jax.nn.sigmoid(dg(rate_low, wru[...], 1, 0))
    unit = k * lax.rsqrt(exact_sum_dot(ones, k * k, 1, 0, True) + 1e-06)
    rate_key = unit * rate
    s_vs[...] = pltpu.roll(v, 64, 1).astype(BF)
    for c in range(chunks):
        s = slice(64 * c, 64 * c + 64)
        f = log_fade[s]
        cumul = exact_sum_dot(tri, f, 1, 0, False)
        end = cumul[63:64]
        ei = jnp.exp(-cumul)
        fo = jnp.exp(end - cumul)
        s_a[s, :] = -unit[s] * jnp.exp(cumul - f)
        s_q[s, :] = q[s] * jnp.exp(cumul)
        s_ki[s, :] = (k[s] * ei).astype(BF)
        s_ri[s, :] = (rate_key[s] * ei).astype(BF)
        s_kf[s, :] = (k[s] * fo).astype(BF)
        s_rf[s, :] = (rate_key[s] * fo).astype(BF)
        s_e[c:c + 1, :] = jnp.exp(end)

    yield
    zb = jnp.zeros((64, 128), BF)
    zf = jnp.zeros((64, 128), F32)

    def only(x, m):
        return jnp.where(m, x, zb if x.dtype == BF else zf)

    right = jnp.logical_not(left)
    cat = jnp.concatenate
    group = 4
    state = jnp.zeros((128, 128), F32)
    for g in range(chunks // group):
        cs = [slice(64 * c, 64 * c + 64) for c in range(g * group, (g + 1) * group)]
        G0, G1, PW, X, VL, VR = [], [], [], [], [], []
        for s in cs:
            a, qq = s_a[s, :].astype(BF), s_q[s, :].astype(BF)
            ki, ri = s_ki[s, :], s_ri[s, :]
            G0.append(dg(cat([only(a, left), only(qq, left)], 0), cat([ri, ki], 0), 1, 1))
            G1.append(dg(cat([only(a, right), only(qq, right)], 0), cat([ki, ri], 0), 1, 1))
        for i, s in enumerate(cs):
            vs = s_vs[s, :]
            VR.append(only(vs, right))
            VL.append(only(vs, left))
            L = cat([only(G0[i][:64], sr), only(G1[i][:64], sl)], 0)
            PW.append(cat([only(G0[i][:64], sl), only(G1[i][:64], sr)], 0))
            a = s_a[s, :]
            X.append(cat([only(a, left), only(a, right)], 0) + bdot(L, cat([VL[i], VR[i]], 0)))
        for it in range(6):
            for i in range(group):
                p16 = PW[i].astype(BF)
                if it < 5:
                    px = dg(p16, cat([p16, X[i].astype(BF)], 1), 1, 0)
                    PW[i] = px[:, :128]
                    X[i] = X[i] + px[:, 128:]
                else:
                    X[i] = X[i] + dg(p16, X[i].astype(BF), 1, 0)
        MM, NN, PC, OO = [], [], [], []
        for i, s in enumerate(cs):
            x16 = X[i].astype(BF)
            h0 = cat([x16[:64], VR[i]], 0)
            h1 = cat([VL[i], x16[64:]], 0)
            y0 = bdot(only(G0[i][64:], upto), h0)
            y1 = bdot(only(G1[i][64:], upto), h1)
            qq = s_q[s, :]
            PC.append(cat([only(y0 + qq, left), only(y1 + qq, right)], 0).astype(BF))
            OO.append(only(y0, right) + only(y1, left))
            kf, rf = s_kf[s, :], s_rf[s, :]
            f = cat([only(rf, left), only(kf, left), only(kf, right), only(rf, right)], 0)
            tr = dg(cat([h0, h1], 0), f, 0, 0)
            e = s_e[g * group + i:g * group + i + 1, :]
            zz = jnp.zeros((128, 128), F32)
            MM.append((jnp.where(same, tr, zz) + jnp.where(eye, e, zz)).astype(BF))
            NN.append(jnp.where(same, zz, tr))
        for i, s in enumerate(cs):
            s16 = state.astype(BF)
            o = dg(PC[i], s16, 1, 1)
            s_o[s, :] = OO[i] + o[:64] + o[64:]
            state = dg(s16, MM[i], 1, 0) + NN[i]
        yield
    o = pltpu.roll(s_o[...], 64, 1)
    centred = o - exact_sum_dot(ones, o, 1, 0, True) * (1.0 / 64)
    spread = exact_sum_dot(ones, centred * centred, 1, 0, True) * (1.0 / 64)
    out[...] = (centred * lax.rsqrt(spread + 0.00064) * gain[...]).astype(BF)


ORDER = (0, 1, 6, 7, 2, 3, 8, 9, 4, 5, 10, 11)


def remote(src, dst, send, recv, **device):
    return pltpu.make_async_remote_copy(
        src_ref=src, dst_ref=dst, send_sem=send, recv_sem=recv, device_id=device,
        device_id_type=MESH)


def meet(peers):
    barrier = pltpu.get_barrier_semaphore()
    for device in peers:
        pl.semaphore_signal(barrier, inc=1, device_id=device, device_id_type=MESH)
    return lambda: pl.semaphore_wait(barrier, len(peers))


def slot_list(ids, z, x):
    row = lax.broadcasted_iota(jnp.int32, (64, 128), 0)
    lane = lax.broadcasted_iota(jnp.int32, (64, 128), 1)
    valid = (row - 8 * (row // 8) < 4) & (lane < 8)
    p = ids.reshape(64, 128).astype(F32)
    plane = jnp.floor((p + 0.5) * (1.0 / 48))
    owner = jnp.floor((p + 0.5) * (1.0 / 12))
    step = owner - 4 * plane - x.astype(F32)
    step = jnp.where(step < 0, step + 4, step)
    slot = step * 12 + p - 12 * owner
    hit = valid & (plane == z.astype(F32))
    m = jnp.where(hit, 1.0, 0.0)
    r1 = lax.broadcasted_iota(jnp.int32, (64, 64), 0)
    c1 = lax.broadcasted_iota(jnp.int32, (64, 64), 1)
    r2 = lax.broadcasted_iota(jnp.int32, (128, 128), 0)
    c2 = lax.broadcasted_iota(jnp.int32, (128, 128), 1)
    near = r1 // 8 == c1 // 8
    above = bdot(jnp.where(near & (c1 < r1), 1.0, 0.0), m)
    column = bdot(jnp.where(near, 1.0, 0.0), m)
    pos = above + bdot(column, jnp.where(r2 < c2, 1.0, 0.0))
    pos = jnp.where(hit, pos, -1.0)
    lanes = lane.astype(F32)
    acc = jnp.zeros((64, 128), F32)
    for b in range(8):
        at = pos[:, b:b + 1]
        acc = acc + jnp.where(at == lanes, slot[:, b:b + 1], 0.0)
        acc = acc + jnp.where((at == lanes - 64) & (at >= 0), b + 1.0, 0.0)
    return jnp.sum(acc.reshape(8, 8, 128), axis=1).astype(jnp.int32)


PIPES = (("st_up", 0, (4, 3, 2, 1)), ("st_down", 1, (4, 5, 6, 7)),
         ("st_up", 1, (3, 2, 1)), ("st_down", 0, (5, 6, 7)))


class Spread:
    def __init__(self, own, buf, send, recv, yp, ym, sib):
        self.copies = []
        for h in range(2):
            s = own.at[pl.ds(256 * h, 256), :]
            links = [(s, buf.at[1, 0, h], sib), (s, buf.at[0, 3, h], yp), (s, buf.at[0, 1, h], ym),
                     (buf.at[0, 3, h], buf.at[1, 3, h], sib), (buf.at[0, 1, h], buf.at[1, 1, h], sib),
                     (buf.at[0, 3, h], buf.at[0, 2, h], yp) if h == 0
                     else (buf.at[0, 1, h], buf.at[0, 2, h], ym),
                     (buf.at[0, 2, h], buf.at[1, 2, h], sib)]
            self.copies.append([
                remote(a, b, send.at[h, k], recv.at[h, k], tp=to) for k, (a, b, to) in enumerate(links)])

    def first(self, h):
        c = self.copies[h]
        for k in ((1, 2, 0) if h == 0 else (2, 1, 0)):
            c[k].start()

    def second(self, h):
        c = self.copies[h]
        if h == 0:
            c[1].wait_recv()
            c[5].start()
            c[3].start()
            c[2].wait_recv()
            c[4].start()
        else:
            c[2].wait_recv()
            c[5].start()
            c[4].start()
            c[1].wait_recv()
            c[3].start()

    def third(self, h):
        self.copies[h][5].wait_recv()
        self.copies[h][6].start()

    def arrived(self, h, *which):
        for k in which:
            self.copies[h][k].wait_recv()

    def finish(self):
        for c in self.copies[0] + self.copies[1]:
            c.wait_send()


def layer_kernel(store, wk, wv, tok, wq, wg, mq, mk, mv, wc, wm, wgu, qgain, ids, wdl, wdu, base, shift, wrl,
                 wru, gain, out,
                 sv, wkv, wvv, tokv, wqv, wgv, mqv, mkv, mvv, wcv, wmv, wguv, kvs, qq, idv, lstv, lst,
                 glow, heads, s_a, s_q, s_ki, s_ri, s_kf, s_rf, s_vs, s_e, s_o,
                 kd, vd, part, den, msg, box, head_all, att, att_all, gate, mixed,
                 in_sem, xs, xr, zs, zr, ids_s, ids_r, ps, pr, hs, hr, as_, ar):
    st, tp = lax.axis_index("st"), lax.axis_index("tp")
    z, x = st // NX, lax.rem(st, NX)
    y, core = tp // 2, lax.rem(tp, 2)
    xp = z * NX + lax.rem(x + 1, NX)
    xm = z * NX + lax.rem(x + NX - 1, NX)
    zp = lax.rem(z + 1, NZ) * NX + x
    zm = lax.rem(z + NZ - 1, NZ) * NX + x
    yp = lax.rem(y + 1, 4) * 2 + core
    ym = lax.rem(y + 3, 4) * 2 + core
    sib = y * 2 + 1 - core
    ready = meet([{"st": xp}, {"st": xm}, {"st": zp}, {"st": zm}, {"tp": yp}, {"tp": ym}, {"tp": sib}])
    loads = {}

    def load(name, src, dst):
        loads[name] = pltpu.make_async_copy(src, dst, in_sem.at[len(loads)])
        loads[name].start()

    load("wk", wk, wkv)
    load("wv", wv, wvv)
    for p, i in enumerate(ORDER):
        load(i, store.at[i], sv.at[p])
    for name, src, dst in (("tok", tok, tokv), ("wq", wq, wqv), ("wg", wg, wgv), ("mq", mq, mqv),
                           ("mk", mk, mkv), ("mv", mv, mvv), ("wm", wm, wmv), ("wgu", wgu, wguv),
                           ("wc", wc, wcv)):
        load(name, src, dst)
    left = [remote(kvs.at[i], kvs.at[12 + i], xs.at[0, i], xr.at[0, i], st=xm) for i in range(12)]
    right = [remote(kvs.at[i], kvs.at[36 + i], xs.at[1, i], xr.at[1, i], st=xp) for i in range(12)]
    hop = [remote(kvs.at[12 + i], kvs.at[24 + i], xs.at[2, i], xr.at[2, i], st=xm) for i in range(6)]
    hop += [remote(kvs.at[36 + i], kvs.at[24 + i], xs.at[2, i], xr.at[2, i], st=xp) for i in range(6, 12)]

    loads["wk"].wait()
    loads["wv"].wait()
    for g in range(3):
        for i in ORDER[4 * g:4 * g + 4]:
            loads[i].wait()
        r = sv[4 * g:4 * g + 4].reshape(384, sv.shape[2])
        k = head_normed(dg(r, wkv[...], 1, 0)).astype(BF)
        v = dg(r, wvv[...], 1, 0).astype(BF)
        for u, i in enumerate(ORDER[4 * g:4 * g + 4]):
            kvs[i, :, 0:256] = k[96 * u:96 * u + 96]
            kvs[i, :, 256:512] = v[96 * u:96 * u + 96]
        if g == 0:
            ready()
        for u in range(2):
            left[2 * g + u].start()
            right[6 + 2 * g + u].start()
    for u in range(6):
        left[6 + u].start()
        right[u].start()
    loads["tok"].wait()
    loads["wq"].wait()
    proj = dg(tokv[...], wqv[...], 1, 0)
    qq[0] = (head_normed(proj) * qgain[...]).astype(BF) * BF(0.0625)
    idv[0] = jnp.zeros((8, 128), jnp.int32)
    idv[0, 0:4, 0:8] = ids[...]

    def rows(ref, s, part):
        return ref if s < 3 else ref.at[pl.ds(256 * part, 256), :]

    up, down, up_ids, down_ids = [], [], [], []
    for s in range(4):
        a, b = (8 - s) % 8, 7 - s
        src = qq.at[a]
        up.append(remote(rows(src, s, 0), rows(qq.at[b], s, 0), zs.at[0, s], zr.at[0, s], st=zp))
        up_ids.append(remote(idv.at[a], idv.at[b], ids_s.at[0, s], ids_r.at[0, s], st=zp))
        src = qq.at[s]
        down.append(remote(rows(src, s, 1), rows(qq.at[s + 1], s, 1), zs.at[1, s], zr.at[1, s], st=zm))
        if s < 3:
            down_ids.append(remote(idv.at[s], idv.at[s + 1], ids_s.at[1, s], ids_r.at[1, s], st=zm))

    def z_start(s):
        up[s].start()
        down[s].start()
        up_ids[s].start()
        if s < 3:
            down_ids[s].start()

    def z_wait(s):
        up[s].wait_recv()
        down[s].wait_recv()
        up_ids[s].wait_recv()
        if s < 3:
            down_ids[s].wait_recv()

    z_start(0)
    for name in ("wg", "mq", "mk", "mv"):
        loads[name].wait()
    glow[...] = dg(tokv[...], wgv[...], 1, 0).astype(BF)
    stages = mixer_stages(tokv, mqv, mkv, mvv, wdl, wdu, base, shift, wrl, wru, gain, heads,
                          s_a, s_q, s_ki, s_ri, s_kf, s_rf, s_vs, s_e, s_o)
    next(stages)
    next(stages)
    z_wait(0)
    z_start(1)
    for _ in stages:
        pass
    hspread = Spread(heads, head_all, hs, hr, yp, ym, sib)
    hspread.first(0)
    hspread.first(1)
    for i in range(6):
        left[i].wait_recv()
        hop[i].start()
        right[6 + i].wait_recv()
        hop[6 + i].start()
    z_wait(1)
    z_start(2)
    hspread.second(0)
    hspread.second(1)
    loads["wgu"].wait()
    loads["wm"].wait()
    loads["wc"].wait()
    gate[...] = jax.nn.sigmoid(dg(glow[...], wguv[...], 1, 0))
    z_wait(2)
    z_start(3)
    hspread.third(0)
    hspread.third(1)
    origin = [[lax.rem(y + r, 4) * 2 + (core if c == 0 else 1 - core) for r in range(4)] for c in range(2)]

    def term(buf, w, size, c, r, h):
        at = pl.multiple_of(origin[c][r] * size, size)
        return dg(buf[c, r, h], w[pl.ds(at, size), :], 1, 0)

    rest = [(c, r) for c in range(2) for r in range(4) if (c, r) != (0, 0)]
    at0 = pl.multiple_of(origin[0][0] * 128, 128)
    for h in range(2):
        hspread.arrived(h, 0, 3, 4, 6)
        m = dg(heads[256 * h:256 * h + 256, :], wmv[pl.ds(at0, 128), :], 1, 0)
        for c, r in rest:
            m = m + term(head_all, wmv, 128, c, r, h)
        mixed[256 * h:256 * h + 256, :] = m
    z_wait(3)
    lstv[...] = slot_list(idv[...], z, x)
    put = pltpu.make_async_copy(lstv, lst, in_sem.at[len(loads)])
    put.start()
    put.wait()
    for i in range(6):
        left[6 + i].wait_recv()
        right[i].wait_recv()
    for c in hop:
        c.wait_recv()
    to = {"st_up": zp, "st_down": zm}
    sends = [[remote(msg.at[p, s], box.at[p, s], ps.at[p, s], pr.at[p, s], st=to[way])
              for s in range(len(ds))] for p, (way, _, ds) in enumerate(PIPES)]

    def own(d, h):
        return part[d, 256 * h:256 * h + 256, :], den[8 * d:8 * d + 8, 0:64]

    lane = lax.broadcasted_iota(jnp.int32, (8, 768), 1)
    r128 = lax.broadcasted_iota(jnp.int32, (128, 768), 0)
    diag = lax.broadcasted_iota(jnp.int32, (64, 128), 0) == lax.broadcasted_iota(jnp.int32, (64, 128), 1)

    def attend(d, n):
        u = n % 2
        block = jnp.zeros((8, 768), jnp.int32)
        for r in range(8):
            e = jnp.minimum(jnp.maximum(lst[d, r], 0), 47)
            kd[u, 96 * r:96 * r + 96, :] = kvs[e, :, 0:256]
            vd[u, 96 * r:96 * r + 96, :] = kvs[e, :, 256:512]
            block = jnp.where((lane >= 96 * r) & (lane < 96 * r + 96), lst[d, 64 + r], block)
        block = block[0:1]
        sums = []
        for t in range(4):
            s = slice(128 * t, 128 * t + 128)
            p = jnp.exp(dg(qq[d, s, :], kd[u], 1, 1))
            p = jnp.where(r128 // 64 + (2 * t + 1) == block, p, 0.0)
            part[d, s, :] = dg(p.astype(BF), vd[u], 1, 0)
            total = jnp.sum(p, axis=1, keepdims=True)
            for v in range(2):
                line = jnp.where(diag, total[64 * v:64 * v + 64], 0.0)
                sums.append(jnp.sum(line, axis=0, keepdims=True))
        den[8 * d:8 * d + 8, :] = jnp.concatenate(sums, axis=0)

    def held(p, s):
        line = box[p, s, 256:272, :].astype(F32)[0:8]
        return box[p, s, 0:256, :].astype(F32), line[:, 0:64] + line[:, 64:128]

    def send(p, s):
        _, h, ds = PIPES[p]
        n, d = own(ds[s], h)
        if s:
            sends[p][s - 1].wait_recv()
            n2, d2 = held(p, s - 1)
            n, d = n + n2, d + d2
        msg[p, s, 0:256, :] = n.astype(BF)
        hi = d.astype(BF).astype(F32)
        line = jnp.concatenate([hi, d - hi, jnp.zeros((8, 128), F32)], axis=1)
        msg[p, s, 256:272, :] = jnp.concatenate([line, jnp.zeros((8, 256), F32)], axis=0).astype(BF)
        sends[p][s].start()

    attend(4, 0)
    send(0, 0)
    send(1, 0)
    attend(3, 1)
    send(2, 0)
    attend(5, 0)
    send(3, 0)
    for n, d in enumerate((2, 6, 1, 7, 0)):
        attend(d, n + 1)
    for p in range(4):
        send(p, 1)
    for p in range(4):
        send(p, 2)
    for p in range(2):
        send(p, 3)
    aspread = Spread(att, att_all, as_, ar, yp, ym, sib)
    for h, pipes in ((0, (3, 0)), (1, (2, 1))):
        n, d = own(0, h)
        for p in pipes:
            s = len(PIPES[p][2]) - 1
            sends[p][s].wait_recv()
            n2, d2 = held(p, s)
            n, d = n + n2, d + d2
        inv = jnp.transpose(1.0 / d)
        for b in range(4):
            col = 4 * h + b
            att[256 * h + 64 * b:256 * h + 64 * b + 64, :] = (
                n[64 * b:64 * b + 64] * inv[:, col:col + 1]).astype(BF)
        aspread.first(h)
    at0 = pl.multiple_of(origin[0][0] * 256, 256)
    acc = [dg(att[256 * h:256 * h + 256, :], wcv[pl.ds(at0, 256), :], 1, 0) for h in range(2)]
    aspread.second(0)
    aspread.second(1)
    for h in range(2):
        aspread.arrived(h, 0)
        for c, r in ((0, 3), (0, 1), (1, 0)):
            acc[h] = acc[h] + term(att_all, wcv, 256, c, r, h)
    aspread.third(0)
    aspread.third(1)
    for h in range(2):
        aspread.arrived(h, 3, 4)
        for c, r in ((0, 2), (1, 1), (1, 3)):
            acc[h] = acc[h] + term(att_all, wcv, 256, c, r, h)
    for h in range(2):
        aspread.arrived(h, 6)
        c = acc[h] + term(att_all, wcv, 256, 1, 2, h)
        s = slice(256 * h, 256 * h + 256)
        out[s, :] = (mixed[s, :] + gate[s, :] * c).astype(BF)
    for line in sends:
        for c in line:
            c.wait_send()
    hspread.finish()
    aspread.finish()


    for c in left + right + hop + up + down + up_ids + down_ids:
        c.wait_send()


def local(
    tokens, mix_query, mix_key, mix_value, decay_lower_map, decay_upper_map, decay_base,
    decay_shift, rate_lower_map, rate_upper_map, norm_gain, mix_out, cross_query, score_gain,
    passage_key, passage_value, cross_out, gate_down, gate_up, store, passage_ids,
):
    rows, width = tokens.shape
    sds = jax.ShapeDtypeStruct
    vm = pltpu.VMEM
    dma = pltpu.SemaphoreType.DMA
    f = lambda: vm((rows, 128), F32)
    b = lambda: vm((rows, 128), BF)
    w256 = lambda: vm((width, 256), BF)
    w128 = lambda: vm((width, 128), BF)
    return pl.pallas_call(
        layer_kernel,
        out_shape=sds((rows, 256), BF),
        in_specs=[ANY] * 12 + [VMEM] * 9,
        out_specs=VMEM,
        scratch_shapes=[
            vm((12, 96, width), BF), w256(), w256(), vm((rows, width), BF), w256(), w128(), w128(),
            w128(), w128(), vm(cross_out.shape, BF), vm(mix_out.shape, BF), vm(gate_up.shape, BF),
            vm((48, 96, 512), BF), vm((NZ, rows, 256), BF), vm((8, 8, 128), jnp.int32),
            vm((8, 128), jnp.int32), pltpu.SMEM((8, 128), jnp.int32), b(), b(),
            f(), f(), b(), b(), b(), b(), b(), vm((8, 128), F32), f(),
            vm((2, 768, 256), BF), vm((2, 768, 256), BF), vm((NZ, rows, 256), F32), vm((64, 128), F32),
            vm((4, 4, 272, 256), BF), vm((4, 4, 272, 256), BF), vm((2, 4, 2, 256, 128), BF),
            vm((rows, 256), BF), vm((2, 4, 2, 256, 256), BF), vm((rows, 256), F32), vm((rows, 256), F32),
            dma((24,)), dma((3, 12)), dma((3, 12)), dma((2, 4)), dma((2, 4)), dma((2, 4)), dma((2, 4)),
            dma((4, 4)), dma((4, 4)), dma((2, 7)), dma((2, 7)), dma((2, 7)), dma((2, 7)),
        ],
        compiler_params=params(62, collective_id=0, has_side_effects=True),
        cost_estimate=cost(3e10),
        name="layer",
    )(store, passage_key, passage_value, tokens, cross_query, gate_down, mix_query, mix_key, mix_value,
      cross_out, mix_out, gate_up, score_gain[None], passage_ids.T, decay_lower_map.T, decay_upper_map,
      decay_base[None], decay_shift.T, rate_lower_map.T, rate_upper_map, norm_gain[None])


def solution(mesh):
    placed = (
        P("st", None), P(None, "tp"), P(None, "tp"), P(None, "tp"), P(), P(None, "tp"), P("tp"),
        P("st", "tp"), P(), P(None, "tp"), P("tp"), P(None, "tp"), P(None, "tp"), P("tp"),
        P(None, "tp"), P(None, "tp"), P(None, "tp"), P(), P(None, "tp"), P("st", None, None),
        P("st", None),
    )
    return jax.shard_map(
        local, mesh=mesh, in_specs=placed, out_specs=P("st", "tp"), check_vma=False)
```

time: 337 us -> 93.8 us (0.28); the launches traced: 332 us -> 93.7 us
  matrix products: 143 us -> 0 us
  Pallas kernels: 0 us -> 92 us
  waiting for transfers between devices: 86.7 us -> 0 us
  local copies, waits for them, and re-layouts: 59.7 us -> 1.67 us
  starting transfers between devices: 17.3 us -> 0 us
  between operations: 13.8 us -> 0.01 us
  other arithmetic: 9.73 us -> 0 us
    dot_general x189 -> x0, matrix products: 143 us -> none  [the longest x32 35.9 us: pair_dots(): return jnp.einsum('hsc,htc->hst', left, right, precision=PRECISE)]
    pallas_call x0 -> x1, Pallas kernels: none -> 92 us  [local(): pl.pallas_call(layer_kernel, out_shape=sds((rows, 256), BF), in_specs=[AN...]
    all_to_all x2 -> x0, waiting for transfers between devices: 55.7 us -> none  [the longest x1 48.7 us: local(): lax.all_to_all(outgoing, 'st', split_axis=0, concat_axis=0, tiled=True)]
    all_gather x2 -> x0, waiting for transfers between devices: 30.9 us -> none  [the longest x1 30.9 us: in_one_piece(): lax.all_gather(both, axis, axis=dim, tiled=True)]
    reshape x8 -> x0, local copies, waits for them, and re-layouts: 18.3 us -> none  [the longest x1 7.17 us: local(): own_rows[served].reshape(owner_count, capacity, row_share, model_width)]
    all_to_all x2 -> x0, starting transfers between devices: 16.8 us -> none  [the longest x1 11.9 us: local(): lax.all_to_all(wanted, 'st', split_axis=0, concat_axis=0, tiled=True)]
    all_gather x1 -> x0, local copies, waits for them, and re-layouts: 14.6 us -> none  [local(): piece = lax.all_gather(picked, 'tp', axis=1, tiled=True)]
    gather x3 -> x0, local copies, waits for them, and re-layouts: 10.6 us -> none  [the longest x2 7.84 us: local(): incoming.reshape(owner_count * capacity, row_share, model_width)[where_from]]
  transfers between devices with their start and end apart: 4 -> 0, of which waited for: 3 -> 0; matrix products, arithmetic and copies ran while one was open for 40% -> 0% of each run, Pallas kernels for 0% -> 0%
where the time goes in v1:
time: 93.8 us; the launch traced here: 93.7 us
  Pallas kernels  92 us (98%)
  local copies, waits for them, and re-layouts  1.67 us (2%)
    pallas_call x1, Pallas kernels, local(): pl.pallas_call(layer_kernel, out_shape=sds((rows, 256), BF), in_specs=[AN...  92 us

profile of v1, /device:TPU:1, one launch (start us, length us, event | category | flops | bytes accessed | tf_op | source)
XLA Modules:
  0.0 93.7 jit_solution(6643362587197509632)
XLA Ops:
  0.0 92.0 %layer.1 = bf16[512,256]{1,0:T(8,128)(2,1)} custom-call(bf16[12,96,2048]{2,1,0:T(8,128)(2,1)} %store.1, bf16[2048,256]{1,0:T(8,128)(2,1)} %wk.1, bf16[2048,256]{1,0:T(8,128)(2,1)} %wv.1, bf16[512,2048]{1,0:T(8,128)(2,1)} %tok.1, bf16[2048,256]{1,0:T(8,128)(2,1)} %wq.1, bf16[2048,128]{1,0:T(8,128)(2,1)} %wg.1, bf16[2048,128]{1,0:T(8,128)(2,1)} %mq.1, ...), custom_call_target="tpu_custom_call" | custom-call | flops 30000001024 | bytes 4000000 | tf_op jit(solution)/shard_map/layer/pallas_call | solution.py:528
  92.0 1.7 %copy.23 = bf16[512,256]{1,0:T(8,128)(2,1)} copy(bf16[512,256]{1,0:T(8,128)(2,1)} %layer.1) | data formatting | bytes 524288

commit v2 on v1

--- a/solution.py
+++ b/solution.py
@@ -253,17 +253,14 @@
         for k in which:
             self.copies[h][k].wait_recv()
 
-    def finish(self):
-        for c in self.copies[0] + self.copies[1]:
-            c.wait_send()
-
 
 def layer_kernel(store, wk, wv, tok, wq, wg, mq, mk, mv, wc, wm, wgu, qgain, ids, wdl, wdu, base, shift, wrl,
                  wru, gain, out,
-                 sv, wkv, wvv, tokv, wqv, wgv, mqv, mkv, mvv, wcv, wmv, wguv, kvs, qq, idv, lstv, lst,
+                 sv, wkv, wvv, tokv, wqv, wgv, mqv, mkv, mvv, wcv, wmv, wguv, ks, vs0, vs1, qq, idv, lstv, lst,
                  glow, heads, s_a, s_q, s_ki, s_ri, s_kf, s_rf, s_vs, s_e, s_o,
-                 kd, vd, part, den, msg, box, head_all, att, att_all, gate, mixed,
-                 in_sem, xs, xr, zs, zr, ids_s, ids_r, ps, pr, hs, hr, as_, ar):
+                 kd, vd, pbuf, part, den, msg, box, head_all, att, att_all, gate, mixed,
+                 in_sem, k_s, k_r, kh_s, kh_r, v_s, v_r, vh_s, vh_r, zs, zr, ids_s, ids_r, ps, pr, sp_s, sp_r):
+    vs = (vs0, vs1)
     st, tp = lax.axis_index("st"), lax.axis_index("tp")
     z, x = st // NX, lax.rem(st, NX)
     y, core = tp // 2, lax.rem(tp, 2)
@@ -281,19 +278,88 @@
         loads[name] = pltpu.make_async_copy(src, dst, in_sem.at[len(loads)])
         loads[name].start()
 
+    load("tok", tok, tokv)
+    load("wq", wq, wqv)
     load("wk", wk, wkv)
     load("wv", wv, wvv)
     for p, i in enumerate(ORDER):
         load(i, store.at[i], sv.at[p])
-    for name, src, dst in (("tok", tok, tokv), ("wq", wq, wqv), ("wg", wg, wgv), ("mq", mq, mqv),
-                           ("mk", mk, mkv), ("mv", mv, mvv), ("wm", wm, wmv), ("wgu", wgu, wguv),
-                           ("wc", wc, wcv)):
+    for name, src, dst in (("wg", wg, wgv), ("mq", mq, mqv), ("mk", mk, mkv), ("mv", mv, mvv),
+                           ("wm", wm, wmv), ("wgu", wgu, wguv), ("wc", wc, wcv)):
         load(name, src, dst)
-    left = [remote(kvs.at[i], kvs.at[12 + i], xs.at[0, i], xr.at[0, i], st=xm) for i in range(12)]
-    right = [remote(kvs.at[i], kvs.at[36 + i], xs.at[1, i], xr.at[1, i], st=xp) for i in range(12)]
-    hop = [remote(kvs.at[12 + i], kvs.at[24 + i], xs.at[2, i], xr.at[2, i], st=xm) for i in range(6)]
-    hop += [remote(kvs.at[36 + i], kvs.at[24 + i], xs.at[2, i], xr.at[2, i], st=xp) for i in range(6, 12)]
-
+
+    left = [remote(ks.at[i], ks.at[12 + i], k_s.at[0, i], k_r.at[0, i], st=xm) for i in range(12)]
+    right = [remote(ks.at[i], ks.at[36 + i], k_s.at[1, i], k_r.at[1, i], st=xp) for i in range(12)]
+
+    def six(ref, at):
+        return ref.at[pl.ds(at, 6)]
+
+    khop = [remote(six(ks, 12), six(ks, 24), kh_s.at[0], kh_r.at[0], st=xm),
+            remote(six(ks, 42), six(ks, 30), kh_s.at[1], kh_r.at[1], st=xp)]
+    vleft = [[remote(six(vs[c], 6 * i), six(vs[c], 12 + 6 * i), v_s.at[c, 0, i], v_r.at[c, 0, i], st=xm)
+              for i in range(2)] for c in range(2)]
+    vright = [[remote(six(vs[c], 6 * i), six(vs[c], 36 + 6 * i), v_s.at[c, 1, i], v_r.at[c, 1, i], st=xp)
+               for i in range(2)] for c in range(2)]
+    vhop = [[remote(six(vs[c], 12), six(vs[c], 24), vh_s.at[c, 0], vh_r.at[c, 0], st=xm),
+             remote(six(vs[c], 42), six(vs[c], 30), vh_s.at[c, 1], vh_r.at[c, 1], st=xp)]
+            for c in range(2)]
+
+    def v_start(c):
+        vleft[c][0].start()
+        vright[c][1].start()
+        vleft[c][1].start()
+        vright[c][0].start()
+
+    def v_hop(c):
+        vleft[c][0].wait_recv()
+        vhop[c][0].start()
+        vright[c][1].wait_recv()
+        vhop[c][1].start()
+
+    def v_wait(c):
+        vleft[c][1].wait_recv()
+        vright[c][0].wait_recv()
+        vhop[c][0].wait_recv()
+        vhop[c][1].wait_recv()
+
+    def rows(ref, s, half):
+        return ref if s < 3 else ref.at[pl.ds(256 * half, 256), :]
+
+    up, down, id_steps = [], [], []
+    for s in range(4):
+        a, b = (8 - s) % 8, 7 - s
+        up.append(remote(rows(qq.at[a], s, 0), rows(qq.at[b], s, 0), zs.at[0, s], zr.at[0, s], st=zp))
+        down.append(remote(rows(qq.at[s], s, 1), rows(qq.at[s + 1], s, 1), zs.at[1, s], zr.at[1, s], st=zm))
+        steps = [remote(idv.at[a], idv.at[b], ids_s.at[0, s], ids_r.at[0, s], st=zp)]
+        if s < 3:
+            steps.append(remote(idv.at[s], idv.at[s + 1], ids_s.at[1, s], ids_r.at[1, s], st=zm))
+        id_steps.append(steps)
+
+    def z_start(s):
+        up[s].start()
+        down[s].start()
+
+    def z_wait(s):
+        up[s].wait_recv()
+        down[s].wait_recv()
+
+    def ids_start(s):
+        for c in id_steps[s]:
+            c.start()
+
+    def ids_wait(s):
+        for c in id_steps[s]:
+            c.wait_recv()
+
+    idv[0] = jnp.zeros((8, 128), jnp.int32)
+    idv[0, 0:4, 0:8] = ids[...]
+    loads["tok"].wait()
+    loads["wq"].wait()
+    proj = dg(tokv[...], wqv[...], 1, 0)
+    qq[0] = (head_normed(proj) * qgain[...]).astype(BF) * BF(0.0625)
+    ready()
+    ids_start(0)
+    z_start(0)
     loads["wk"].wait()
     loads["wv"].wait()
     for g in range(3):
@@ -301,127 +367,69 @@
             loads[i].wait()
         r = sv[4 * g:4 * g + 4].reshape(384, sv.shape[2])
         k = head_normed(dg(r, wkv[...], 1, 0)).astype(BF)
-        v = dg(r, wvv[...], 1, 0).astype(BF)
         for u, i in enumerate(ORDER[4 * g:4 * g + 4]):
-            kvs[i, :, 0:256] = k[96 * u:96 * u + 96]
-            kvs[i, :, 256:512] = v[96 * u:96 * u + 96]
-        if g == 0:
-            ready()
+            ks[i] = k[96 * u:96 * u + 96]
         for u in range(2):
             left[2 * g + u].start()
             right[6 + 2 * g + u].start()
     for u in range(6):
         left[6 + u].start()
         right[u].start()
-    loads["tok"].wait()
-    loads["wq"].wait()
-    proj = dg(tokv[...], wqv[...], 1, 0)
-    qq[0] = (head_normed(proj) * qgain[...]).astype(BF) * BF(0.0625)
-    idv[0] = jnp.zeros((8, 128), jnp.int32)
-    idv[0, 0:4, 0:8] = ids[...]
-
-    def rows(ref, s, part):
-        return ref if s < 3 else ref.at[pl.ds(256 * part, 256), :]
-
-    up, down, up_ids, down_ids = [], [], [], []
-    for s in range(4):
-        a, b = (8 - s) % 8, 7 - s
-        src = qq.at[a]
-        up.append(remote(rows(src, s, 0), rows(qq.at[b], s, 0), zs.at[0, s], zr.at[0, s], st=zp))
-        up_ids.append(remote(idv.at[a], idv.at[b], ids_s.at[0, s], ids_r.at[0, s], st=zp))
-        src = qq.at[s]
-        down.append(remote(rows(src, s, 1), rows(qq.at[s + 1], s, 1), zs.at[1, s], zr.at[1, s], st=zm))
-        if s < 3:
-            down_ids.append(remote(idv.at[s], idv.at[s + 1], ids_s.at[1, s], ids_r.at[1, s], st=zm))
-
-    def z_start(s):
-        up[s].start()
-        down[s].start()
-        up_ids[s].start()
-        if s < 3:
-            down_ids[s].start()
-
-    def z_wait(s):
-        up[s].wait_recv()
-        down[s].wait_recv()
-        up_ids[s].wait_recv()
-        if s < 3:
-            down_ids[s].wait_recv()
-
-    z_start(0)
+    ids_wait(0)
+    ids_start(1)
+    for g in range(3):
+        v = dg(sv[4 * g:4 * g + 4].reshape(384, sv.shape[2]), wvv[...], 1, 0).astype(BF)
+        for u, i in enumerate(ORDER[4 * g:4 * g + 4]):
+            vs0[i] = v[96 * u:96 * u + 96, 0:128]
+            vs1[i] = v[96 * u:96 * u + 96, 128:256]
+    ids_wait(1)
+    ids_start(2)
     for name in ("wg", "mq", "mk", "mv"):
         loads[name].wait()
     glow[...] = dg(tokv[...], wgv[...], 1, 0).astype(BF)
     stages = mixer_stages(tokv, mqv, mkv, mvv, wdl, wdu, base, shift, wrl, wru, gain, heads,
                           s_a, s_q, s_ki, s_ri, s_kf, s_rf, s_vs, s_e, s_o)
     next(stages)
-    next(stages)
     z_wait(0)
     z_start(1)
+    ids_wait(2)
+    ids_start(3)
+    next(stages)
+    for i in range(6):
+        left[i].wait_recv()
+    khop[0].start()
+    for i in range(6):
+        right[6 + i].wait_recv()
+    khop[1].start()
+    v_start(0)
     for _ in stages:
         pass
-    hspread = Spread(heads, head_all, hs, hr, yp, ym, sib)
+    ids_wait(3)
+    lstv[...] = slot_list(idv[...], z, x)
+    put = pltpu.make_async_copy(lstv, lst, in_sem.at[len(loads)])
+    put.start()
+    z_wait(1)
+    z_start(2)
+    hspread = Spread(heads, head_all, sp_s.at[0], sp_r.at[0], yp, ym, sib)
     hspread.first(0)
     hspread.first(1)
-    for i in range(6):
-        left[i].wait_recv()
-        hop[i].start()
-        right[6 + i].wait_recv()
-        hop[6 + i].start()
-    z_wait(1)
-    z_start(2)
-    hspread.second(0)
-    hspread.second(1)
     loads["wgu"].wait()
     loads["wm"].wait()
     loads["wc"].wait()
     gate[...] = jax.nn.sigmoid(dg(glow[...], wguv[...], 1, 0))
-    z_wait(2)
-    z_start(3)
-    hspread.third(0)
-    hspread.third(1)
-    origin = [[lax.rem(y + r, 4) * 2 + (core if c == 0 else 1 - core) for r in range(4)] for c in range(2)]
-
-    def term(buf, w, size, c, r, h):
-        at = pl.multiple_of(origin[c][r] * size, size)
-        return dg(buf[c, r, h], w[pl.ds(at, size), :], 1, 0)
-
-    rest = [(c, r) for c in range(2) for r in range(4) if (c, r) != (0, 0)]
-    at0 = pl.multiple_of(origin[0][0] * 128, 128)
-    for h in range(2):
-        hspread.arrived(h, 0, 3, 4, 6)
-        m = dg(heads[256 * h:256 * h + 256, :], wmv[pl.ds(at0, 128), :], 1, 0)
-        for c, r in rest:
-            m = m + term(head_all, wmv, 128, c, r, h)
-        mixed[256 * h:256 * h + 256, :] = m
-    z_wait(3)
-    lstv[...] = slot_list(idv[...], z, x)
-    put = pltpu.make_async_copy(lstv, lst, in_sem.at[len(loads)])
-    put.start()
     put.wait()
-    for i in range(6):
-        left[6 + i].wait_recv()
-        right[i].wait_recv()
-    for c in hop:
-        c.wait_recv()
-    to = {"st_up": zp, "st_down": zm}
-    sends = [[remote(msg.at[p, s], box.at[p, s], ps.at[p, s], pr.at[p, s], st=to[way])
-              for s in range(len(ds))] for p, (way, _, ds) in enumerate(PIPES)]
-
-    def own(d, h):
-        return part[d, 256 * h:256 * h + 256, :], den[8 * d:8 * d + 8, 0:64]
 
     lane = lax.broadcasted_iota(jnp.int32, (8, 768), 1)
     r128 = lax.broadcasted_iota(jnp.int32, (128, 768), 0)
     diag = lax.broadcasted_iota(jnp.int32, (64, 128), 0) == lax.broadcasted_iota(jnp.int32, (64, 128), 1)
 
-    def attend(d, n):
-        u = n % 2
+    def slot(d, r):
+        return jnp.minimum(jnp.maximum(lst[d, r], 0), 47)
+
+    def scores(d, u):
         block = jnp.zeros((8, 768), jnp.int32)
         for r in range(8):
-            e = jnp.minimum(jnp.maximum(lst[d, r], 0), 47)
-            kd[u, 96 * r:96 * r + 96, :] = kvs[e, :, 0:256]
-            vd[u, 96 * r:96 * r + 96, :] = kvs[e, :, 256:512]
+            kd[u, 96 * r:96 * r + 96, :] = ks[slot(d, r)]
             block = jnp.where((lane >= 96 * r) & (lane < 96 * r + 96), lst[d, 64 + r], block)
         block = block[0:1]
         sums = []
@@ -429,87 +437,166 @@
             s = slice(128 * t, 128 * t + 128)
             p = jnp.exp(dg(qq[d, s, :], kd[u], 1, 1))
             p = jnp.where(r128 // 64 + (2 * t + 1) == block, p, 0.0)
-            part[d, s, :] = dg(p.astype(BF), vd[u], 1, 0)
+            pbuf[d, s, :] = p.astype(BF)
             total = jnp.sum(p, axis=1, keepdims=True)
             for v in range(2):
                 line = jnp.where(diag, total[64 * v:64 * v + 64], 0.0)
                 sums.append(jnp.sum(line, axis=0, keepdims=True))
         den[8 * d:8 * d + 8, :] = jnp.concatenate(sums, axis=0)
 
-    def held(p, s):
-        line = box[p, s, 256:272, :].astype(F32)[0:8]
-        return box[p, s, 0:256, :].astype(F32), line[:, 0:64] + line[:, 64:128]
-
-    def send(p, s):
+    def values(c, d, u):
+        for r in range(8):
+            vd[u, 96 * r:96 * r + 96, :] = vs[c][slot(d, r)]
+        part[c, d] = dg(pbuf[d], vd[u], 1, 0)
+
+    for i in range(6):
+        left[6 + i].wait_recv()
+        right[i].wait_recv()
+    khop[0].wait_recv()
+    khop[1].wait_recv()
+    for n, d in enumerate((0, 1, 7, 2, 6)):
+        scores(d, n % 2)
+    z_wait(2)
+    z_start(3)
+    scores(3, 1)
+    scores(5, 0)
+    v_hop(0)
+    v_start(1)
+    hspread.second(0)
+    hspread.second(1)
+    origin = [[lax.rem(y + r, 4) * 2 + (core if c == 0 else 1 - core) for r in range(4)] for c in range(2)]
+    rest = [(c, r) for c in range(2) for r in range(4) if (c, r) != (0, 0)]
+
+    def weight(w, size, c, r, shift_rows):
+        at = pl.multiple_of(origin[c][r] * size + shift_rows, 128)
+        return w[pl.ds(at, 128), :]
+
+    hspread.third(0)
+    hspread.third(1)
+    z_wait(3)
+    scores(4, 1)
+    for h in range(2):
+        hspread.arrived(h, 0, 3, 4, 6)
+        m = dg(heads[256 * h:256 * h + 256, :], weight(wmv, 128, 0, 0, 0), 1, 0)
+        for c, r in rest:
+            m = m + dg(head_all[c, r, h], weight(wmv, 128, c, r, 0), 1, 0)
+        mixed[256 * h:256 * h + 256, :] = m
+
+    to = {"st_up": zp, "st_down": zm}
+
+    def box_rows(ref, c, p, s):
+        return ref.at[c, p, s] if c == 0 else ref.at[c, p, s, pl.ds(0, 256), :]
+
+    sends = [[[remote(box_rows(msg, c, p, s), box_rows(box, c, p, s), ps.at[c, p, s], pr.at[c, p, s], st=to[way])
+               for s in range(len(ds))] for p, (way, _, ds) in enumerate(PIPES)] for c in range(2)]
+
+    def own(c, d, h):
+        return part[c, d, 256 * h:256 * h + 256, :], den[8 * d:8 * d + 8, 0:64]
+
+    def held(c, p, s):
+        n = box[c, p, s, 0:256, :].astype(F32)
+        if c == 1:
+            return n, 0.0
+        line = box[c, p, s, 256:272, :].astype(F32)[0:8]
+        return n, line[:, 0:64] + line[:, 64:128]
+
+    def send(c, p, s):
         _, h, ds = PIPES[p]
-        n, d = own(ds[s], h)
+        n, d = own(c, ds[s], h)
         if s:
-            sends[p][s - 1].wait_recv()
-            n2, d2 = held(p, s - 1)
+            sends[c][p][s - 1].wait_recv()
+            n2, d2 = held(c, p, s - 1)
             n, d = n + n2, d + d2
-        msg[p, s, 0:256, :] = n.astype(BF)
-        hi = d.astype(BF).astype(F32)
-        line = jnp.concatenate([hi, d - hi, jnp.zeros((8, 128), F32)], axis=1)
-        msg[p, s, 256:272, :] = jnp.concatenate([line, jnp.zeros((8, 256), F32)], axis=0).astype(BF)
-        sends[p][s].start()
-
-    attend(4, 0)
-    send(0, 0)
-    send(1, 0)
-    attend(3, 1)
-    send(2, 0)
-    attend(5, 0)
-    send(3, 0)
-    for n, d in enumerate((2, 6, 1, 7, 0)):
-        attend(d, n + 1)
-    for p in range(4):
-        send(p, 1)
-    for p in range(4):
-        send(p, 2)
-    for p in range(2):
-        send(p, 3)
-    aspread = Spread(att, att_all, as_, ar, yp, ym, sib)
-    for h, pipes in ((0, (3, 0)), (1, (2, 1))):
-        n, d = own(0, h)
-        for p in pipes:
-            s = len(PIPES[p][2]) - 1
-            sends[p][s].wait_recv()
-            n2, d2 = held(p, s)
-            n, d = n + n2, d + d2
-        inv = jnp.transpose(1.0 / d)
-        for b in range(4):
-            col = 4 * h + b
-            att[256 * h + 64 * b:256 * h + 64 * b + 64, :] = (
-                n[64 * b:64 * b + 64] * inv[:, col:col + 1]).astype(BF)
-        aspread.first(h)
-    at0 = pl.multiple_of(origin[0][0] * 256, 256)
-    acc = [dg(att[256 * h:256 * h + 256, :], wcv[pl.ds(at0, 256), :], 1, 0) for h in range(2)]
-    aspread.second(0)
-    aspread.second(1)
+        msg[c, p, s, 0:256, :] = n.astype(BF)
+        if c == 0:
+            hi = d.astype(BF).astype(F32)
+            line = jnp.concatenate([hi, d - hi], axis=1)
+            msg[c, p, s, 256:272, :] = jnp.concatenate([line, jnp.zeros((8, 128), F32)], axis=0).astype(BF)
+        sends[c][p][s].start()
+
+    inverse = [None, None]
+    spread = [Spread(att.at[c], att_all.at[c], sp_s.at[1 + c], sp_r.at[1 + c], yp, ym, sib) for c in range(2)]
+
+    def settle(c):
+        for h, pipes in ((0, (3, 0)), (1, (2, 1))):
+            n, d = own(c, 0, h)
+            for p in pipes:
+                s = len(PIPES[p][2]) - 1
+                sends[c][p][s].wait_recv()
+                n2, d2 = held(c, p, s)
+                n, d = n + n2, d + d2
+            if c == 0:
+                inverse[h] = jnp.transpose(1.0 / d)
+            for b in range(4):
+                col = 4 * h + b
+                att[c, 256 * h + 64 * b:256 * h + 64 * b + 64, :] = (
+                    n[64 * b:64 * b + 64] * inverse[h][:, col:col + 1]).astype(BF)
+            spread[c].first(h)
+
+    def begin(c):
+        values(c, 4, 0)
+        send(c, 0, 0)
+        send(c, 1, 0)
+        values(c, 3, 1)
+        send(c, 2, 0)
+        values(c, 5, 0)
+        send(c, 3, 0)
+        for n, d in enumerate((2, 6, 1, 7, 0)):
+            values(c, d, (n + 1) % 2)
+
+    def step(c, s):
+        for p in range(4):
+            if s < len(PIPES[p][2]):
+                send(c, p, s)
+
+    def add(acc, c, h, which):
+        for q, r in which:
+            acc = acc + dg(att_all[c, q, r, h], weight(wcv, 256, q, r, 128 * c), 1, 0)
+        return acc
+
+    v_wait(0)
+    begin(0)
+    v_hop(1)
+    step(0, 1)
+    step(0, 2)
+    v_wait(1)
+    begin(1)
+    step(0, 3)
+    step(1, 1)
+    settle(0)
+    step(1, 2)
+    spread[0].second(0)
+    spread[0].second(1)
+    step(1, 3)
+    spread[0].third(0)
+    spread[0].third(1)
+    acc = []
     for h in range(2):
-        aspread.arrived(h, 0)
-        for c, r in ((0, 3), (0, 1), (1, 0)):
-            acc[h] = acc[h] + term(att_all, wcv, 256, c, r, h)
-    aspread.third(0)
-    aspread.third(1)
+        a = dg(att[0, 256 * h:256 * h + 256, :], weight(wcv, 256, 0, 0, 0), 1, 0)
+        spread[0].arrived(h, 0, 3, 4, 6)
+        acc.append(add(a, 0, h, rest))
+    settle(1)
     for h in range(2):
-        aspread.arrived(h, 3, 4)
-        for c, r in ((0, 2), (1, 1), (1, 3)):
-            acc[h] = acc[h] + term(att_all, wcv, 256, c, r, h)
+        acc[h] = acc[h] + dg(att[1, 256 * h:256 * h + 256, :], weight(wcv, 256, 0, 0, 128), 1, 0)
+    spread[1].second(0)
+    spread[1].second(1)
     for h in range(2):
-        aspread.arrived(h, 6)
-        c = acc[h] + term(att_all, wcv, 256, 1, 2, h)
+        spread[1].arrived(h, 0)
+        acc[h] = add(acc[h], 1, h, ((0, 3), (0, 1), (1, 0)))
+    spread[1].third(0)
+    spread[1].third(1)
+    for h in range(2):
+        spread[1].arrived(h, 3, 4)
+        acc[h] = add(acc[h], 1, h, ((0, 2), (1, 1), (1, 3)))
+    for h in range(2):
+        spread[1].arrived(h, 6)
+        c = add(acc[h], 1, h, ((1, 2),))
         s = slice(256 * h, 256 * h + 256)
         out[s, :] = (mixed[s, :] + gate[s, :] * c).astype(BF)
-    for line in sends:
-        for c in line:
+    for group in (left, right, khop, *vleft, *vright, *vhop, up, down, *id_steps,
+                  *sends[0], *sends[1], *(p for sp in (hspread, *spread) for p in sp.copies)):
+        for c in group:
             c.wait_send()
-    hspread.finish()
-    aspread.finish()
-
-
-    for c in left + right + hop + up + down + up_ids + down_ids:
-        c.wait_send()
 
 
 def local(
@@ -533,14 +620,16 @@
         scratch_shapes=[
             vm((12, 96, width), BF), w256(), w256(), vm((rows, width), BF), w256(), w128(), w128(),
             w128(), w128(), vm(cross_out.shape, BF), vm(mix_out.shape, BF), vm(gate_up.shape, BF),
-            vm((48, 96, 512), BF), vm((NZ, rows, 256), BF), vm((8, 8, 128), jnp.int32),
-            vm((8, 128), jnp.int32), pltpu.SMEM((8, 128), jnp.int32), b(), b(),
+            vm((48, 96, 256), BF), vm((48, 96, 128), BF), vm((48, 96, 128), BF), vm((NZ, rows, 256), BF),
+            vm((8, 8, 128), jnp.int32), vm((8, 128), jnp.int32), pltpu.SMEM((8, 128), jnp.int32), b(), b(),
             f(), f(), b(), b(), b(), b(), b(), vm((8, 128), F32), f(),
-            vm((2, 768, 256), BF), vm((2, 768, 256), BF), vm((NZ, rows, 256), F32), vm((64, 128), F32),
-            vm((4, 4, 272, 256), BF), vm((4, 4, 272, 256), BF), vm((2, 4, 2, 256, 128), BF),
-            vm((rows, 256), BF), vm((2, 4, 2, 256, 256), BF), vm((rows, 256), F32), vm((rows, 256), F32),
-            dma((24,)), dma((3, 12)), dma((3, 12)), dma((2, 4)), dma((2, 4)), dma((2, 4)), dma((2, 4)),
-            dma((4, 4)), dma((4, 4)), dma((2, 7)), dma((2, 7)), dma((2, 7)), dma((2, 7)),
+            vm((2, 768, 256), BF), vm((2, 768, 128), BF), vm((NZ, rows, 768), BF),
+            vm((2, NZ, rows, 128), F32), vm((64, 128), F32),
+            vm((2, 4, 4, 272, 128), BF), vm((2, 4, 4, 272, 128), BF), vm((2, 4, 2, 256, 128), BF),
+            vm((2, rows, 128), BF), vm((2, 2, 4, 2, 256, 128), BF), vm((rows, 256), F32), vm((rows, 256), F32),
+            dma((24,)), dma((2, 12)), dma((2, 12)), dma((2,)), dma((2,)), dma((2, 2, 2)), dma((2, 2, 2)),
+            dma((2, 2)), dma((2, 2)), dma((2, 4)), dma((2, 4)), dma((2, 4)), dma((2, 4)),
+            dma((2, 4, 4)), dma((2, 4, 4)), dma((3, 2, 7)), dma((3, 2, 7)),
         ],
         compiler_params=params(62, collective_id=0, has_side_effects=True),
         cost_estimate=cost(3e10),

time: 93.8 us -> 92.1 us (0.982)
  Pallas kernels: 92 us -> 90.3 us
    pallas_call x1, Pallas kernels: 92 us -> 90.3 us  [local(): pl.pallas_call(layer_kernel, out_shape=sds((rows, 256), BF), in_specs=[AN...]
where the time goes in v2:
time: 92.1 us; the launch traced here: 92 us
  Pallas kernels  90.3 us (98%)
  local copies, waits for them, and re-layouts  1.67 us (2%)
    pallas_call x1, Pallas kernels, local(): pl.pallas_call(layer_kernel, out_shape=sds((rows, 256), BF), in_specs=[AN...  90.3 us

profile of v2, /device:TPU:1, one launch (start us, length us, event | category | flops | bytes accessed | tf_op | source)
XLA Modules:
  0.0 92.0 jit_solution(6638830053960441046)
XLA Ops:
  0.0 90.3 %layer.1 = bf16[512,256]{1,0:T(8,128)(2,1)} custom-call(bf16[12,96,2048]{2,1,0:T(8,128)(2,1)} %store.1, bf16[2048,256]{1,0:T(8,128)(2,1)} %wk.1, bf16[2048,256]{1,0:T(8,128)(2,1)} %wv.1, bf16[512,2048]{1,0:T(8,128)(2,1)} %tok.1, bf16[2048,256]{1,0:T(8,128)(2,1)} %wq.1, bf16[2048,128]{1,0:T(8,128)(2,1)} %wg.1, bf16[2048,128]{1,0:T(8,128)(2,1)} %mq.1, ...), custom_call_target="tpu_custom_call" | custom-call | flops 30000001024 | bytes 4000000 | tf_op jit(solution)/shard_map/layer/pallas_call | solution.py:615
  90.3 1.7 %copy.23 = bf16[512,256]{1,0:T(8,128)(2,1)} copy(bf16[512,256]{1,0:T(8,128)(2,1)} %layer.1) | data formatting | bytes 524288

commit v3 on v2

--- a/solution.py
+++ b/solution.py
@@ -79,6 +79,7 @@
     log_fade = jax.nn.sigmoid(pre) * (-math.exp(-0.5))
     rate_low = dg(t, wrl[...], 1, 1).astype(BF)
     rate = jax.nn.sigmoid(dg(rate_low, wru[...], 1, 0))
+    yield
     unit = k * lax.rsqrt(exact_sum_dot(ones, k * k, 1, 0, True) + 1e-06)
     rate_key = unit * rate
     s_vs[...] = pltpu.roll(v, 64, 1).astype(BF)
@@ -288,11 +289,13 @@
                            ("wm", wm, wmv), ("wgu", wgu, wguv), ("wc", wc, wcv)):
         load(name, src, dst)
 
-    left = [remote(ks.at[i], ks.at[12 + i], k_s.at[0, i], k_r.at[0, i], st=xm) for i in range(12)]
-    right = [remote(ks.at[i], ks.at[36 + i], k_s.at[1, i], k_r.at[1, i], st=xp) for i in range(12)]
-
-    def six(ref, at):
-        return ref.at[pl.ds(at, 6)]
+    def six(ref, at, n=6):
+        return ref.at[pl.ds(at, n)]
+
+    left = [remote(six(ks, a, n), six(ks, 12 + a, n), k_s.at[0, i], k_r.at[0, i], st=xm)
+            for i, (a, n) in enumerate(((0, 2), (2, 2), (4, 2), (6, 6)))]
+    right = [remote(six(ks, a, n), six(ks, 36 + a, n), k_s.at[1, i], k_r.at[1, i], st=xp)
+             for i, (a, n) in enumerate(((6, 2), (8, 2), (10, 2), (0, 6)))]
 
     khop = [remote(six(ks, 12), six(ks, 24), kh_s.at[0], kh_r.at[0], st=xm),
             remote(six(ks, 42), six(ks, 30), kh_s.at[1], kh_r.at[1], st=xp)]
@@ -369,12 +372,10 @@
         k = head_normed(dg(r, wkv[...], 1, 0)).astype(BF)
         for u, i in enumerate(ORDER[4 * g:4 * g + 4]):
             ks[i] = k[96 * u:96 * u + 96]
-        for u in range(2):
-            left[2 * g + u].start()
-            right[6 + 2 * g + u].start()
-    for u in range(6):
-        left[6 + u].start()
-        right[u].start()
+        left[g].start()
+        right[g].start()
+    left[3].start()
+    right[3].start()
     ids_wait(0)
     ids_start(1)
     for g in range(3):
@@ -390,26 +391,28 @@
     stages = mixer_stages(tokv, mqv, mkv, mvv, wdl, wdu, base, shift, wrl, wru, gain, heads,
                           s_a, s_q, s_ki, s_ri, s_kf, s_rf, s_vs, s_e, s_o)
     next(stages)
+    ids_wait(2)
+    ids_start(3)
     z_wait(0)
     z_start(1)
-    ids_wait(2)
-    ids_start(3)
     next(stages)
-    for i in range(6):
+    for i in range(3):
         left[i].wait_recv()
     khop[0].start()
-    for i in range(6):
-        right[6 + i].wait_recv()
+    for i in range(3):
+        right[i].wait_recv()
     khop[1].start()
     v_start(0)
-    for _ in stages:
-        pass
+    next(stages)
     ids_wait(3)
     lstv[...] = slot_list(idv[...], z, x)
     put = pltpu.make_async_copy(lstv, lst, in_sem.at[len(loads)])
     put.start()
+    next(stages)
     z_wait(1)
     z_start(2)
+    for _ in stages:
+        pass
     hspread = Spread(heads, head_all, sp_s.at[0], sp_r.at[0], yp, ym, sib)
     hspread.first(0)
     hspread.first(1)
@@ -449,21 +452,22 @@
             vd[u, 96 * r:96 * r + 96, :] = vs[c][slot(d, r)]
         part[c, d] = dg(pbuf[d], vd[u], 1, 0)
 
-    for i in range(6):
-        left[6 + i].wait_recv()
-        right[i].wait_recv()
+    hspread.second(0)
+    hspread.second(1)
+    left[3].wait_recv()
+    right[3].wait_recv()
     khop[0].wait_recv()
     khop[1].wait_recv()
-    for n, d in enumerate((0, 1, 7, 2, 6)):
+    for n, d in enumerate((0, 1, 7)):
         scores(d, n % 2)
     z_wait(2)
     z_start(3)
+    scores(2, 1)
+    v_hop(0)
+    v_start(1)
+    scores(6, 0)
     scores(3, 1)
     scores(5, 0)
-    v_hop(0)
-    v_start(1)
-    hspread.second(0)
-    hspread.second(1)
     origin = [[lax.rem(y + r, 4) * 2 + (core if c == 0 else 1 - core) for r in range(4)] for c in range(2)]
     rest = [(c, r) for c in range(2) for r in range(4) if (c, r) != (0, 0)]
 
@@ -627,7 +631,7 @@
             vm((2, NZ, rows, 128), F32), vm((64, 128), F32),
             vm((2, 4, 4, 272, 128), BF), vm((2, 4, 4, 272, 128), BF), vm((2, 4, 2, 256, 128), BF),
             vm((2, rows, 128), BF), vm((2, 2, 4, 2, 256, 128), BF), vm((rows, 256), F32), vm((rows, 256), F32),
-            dma((24,)), dma((2, 12)), dma((2, 12)), dma((2,)), dma((2,)), dma((2, 2, 2)), dma((2, 2, 2)),
+            dma((24,)), dma((2, 4)), dma((2, 4)), dma((2,)), dma((2,)), dma((2, 2, 2)), dma((2, 2, 2)),
             dma((2, 2)), dma((2, 2)), dma((2, 4)), dma((2, 4)), dma((2, 4)), dma((2, 4)),
             dma((2, 4, 4)), dma((2, 4, 4)), dma((3, 2, 7)), dma((3, 2, 7)),
         ],

time: 92.1 us -> 91.8 us (level)
  no operation moved by 1% of the time
where the time goes in v3:
time: 91.8 us; the launch traced here: 91.7 us
  Pallas kernels  90 us (98%)
  local copies, waits for them, and re-layouts  1.67 us (2%)
    pallas_call x1, Pallas kernels, local(): pl.pallas_call(layer_kernel, out_shape=sds((rows, 256), BF), in_specs=[AN...  90 us

profile of v3, /device:TPU:1, one launch (start us, length us, event | category | flops | bytes accessed | tf_op | source)
XLA Modules:
  0.0 91.7 jit_solution(5226681460679080776)
XLA Ops:
  0.0 90.0 %layer.1 = bf16[512,256]{1,0:T(8,128)(2,1)} custom-call(bf16[12,96,2048]{2,1,0:T(8,128)(2,1)} %store.1, bf16[2048,256]{1,0:T(8,128)(2,1)} %wk.1, bf16[2048,256]{1,0:T(8,128)(2,1)} %wv.1, bf16[512,2048]{1,0:T(8,128)(2,1)} %tok.1, bf16[2048,256]{1,0:T(8,128)(2,1)} %wq.1, bf16[2048,128]{1,0:T(8,128)(2,1)} %wg.1, bf16[2048,128]{1,0:T(8,128)(2,1)} %mq.1, ...), custom_call_target="tpu_custom_call" | custom-call | flops 30000001024 | bytes 4000000 | tf_op jit(solution)/shard_map/layer/pallas_call | solution.py:619
  90.0 1.7 %copy.23 = bf16[512,256]{1,0:T(8,128)(2,1)} copy(bf16[512,256]{1,0:T(8,128)(2,1)} %layer.1) | data formatting | bytes 524288

commit v4 on v3

--- a/solution.py
+++ b/solution.py
@@ -325,26 +325,33 @@
         vhop[c][0].wait_recv()
         vhop[c][1].wait_recv()
 
-    def rows(ref, s, half):
-        return ref if s < 3 else ref.at[pl.ds(256 * half, 256), :]
-
-    up, down, id_steps = [], [], []
+    pieces, id_steps = {}, []
     for s in range(4):
         a, b = (8 - s) % 8, 7 - s
-        up.append(remote(rows(qq.at[a], s, 0), rows(qq.at[b], s, 0), zs.at[0, s], zr.at[0, s], st=zp))
-        down.append(remote(rows(qq.at[s], s, 1), rows(qq.at[s + 1], s, 1), zs.at[1, s], zr.at[1, s], st=zm))
+        for h in range(2):
+            at = pl.ds(256 * h, 256)
+            both = []
+            if s < 3 or h == 0:
+                both.append(remote(qq.at[a, at, :], qq.at[b, at, :], zs.at[0, s, h], zr.at[0, s, h], st=zp))
+            if s < 3 or h == 1:
+                both.append(remote(qq.at[s, at, :], qq.at[s + 1, at, :], zs.at[1, s, h], zr.at[1, s, h], st=zm))
+            pieces[s, h] = both
         steps = [remote(idv.at[a], idv.at[b], ids_s.at[0, s], ids_r.at[0, s], st=zp)]
         if s < 3:
             steps.append(remote(idv.at[s], idv.at[s + 1], ids_s.at[1, s], ids_r.at[1, s], st=zm))
         id_steps.append(steps)
 
-    def z_start(s):
-        up[s].start()
-        down[s].start()
-
-    def z_wait(s):
-        up[s].wait_recv()
-        down[s].wait_recv()
+    def z_start(s, h):
+        for c in pieces[s, h]:
+            c.start()
+
+    def z_wait(s, h):
+        for c in pieces[s, h]:
+            c.wait_recv()
+
+    def z_pass(s, h):
+        z_wait(s, h)
+        z_start(s + 1, h)
 
     def ids_start(s):
         for c in id_steps[s]:
@@ -362,7 +369,8 @@
     qq[0] = (head_normed(proj) * qgain[...]).astype(BF) * BF(0.0625)
     ready()
     ids_start(0)
-    z_start(0)
+    z_start(0, 0)
+    z_start(0, 1)
     loads["wk"].wait()
     loads["wv"].wait()
     for g in range(3):
@@ -390,12 +398,16 @@
     glow[...] = dg(tokv[...], wgv[...], 1, 0).astype(BF)
     stages = mixer_stages(tokv, mqv, mkv, mvv, wdl, wdu, base, shift, wrl, wru, gain, heads,
                           s_a, s_q, s_ki, s_ri, s_kf, s_rf, s_vs, s_e, s_o)
-    next(stages)
     ids_wait(2)
     ids_start(3)
-    z_wait(0)
-    z_start(1)
+    z_pass(0, 0)
     next(stages)
+    z_pass(0, 1)
+    next(stages)
+    ids_wait(3)
+    lstv[...] = slot_list(idv[...], z, x)
+    put = pltpu.make_async_copy(lstv, lst, in_sem.at[len(loads)])
+    put.start()
     for i in range(3):
         left[i].wait_recv()
     khop[0].start()
@@ -403,14 +415,11 @@
         right[i].wait_recv()
     khop[1].start()
     v_start(0)
+    z_pass(1, 0)
     next(stages)
-    ids_wait(3)
-    lstv[...] = slot_list(idv[...], z, x)
-    put = pltpu.make_async_copy(lstv, lst, in_sem.at[len(loads)])
-    put.start()
+    z_pass(1, 1)
     next(stages)
-    z_wait(1)
-    z_start(2)
+    z_pass(2, 0)
     for _ in stages:
         pass
     hspread = Spread(heads, head_all, sp_s.at[0], sp_r.at[0], yp, ym, sib)
@@ -421,6 +430,7 @@
     loads["wc"].wait()
     gate[...] = jax.nn.sigmoid(dg(glow[...], wguv[...], 1, 0))
     put.wait()
+    z_pass(2, 1)
 
     lane = lax.broadcasted_iota(jnp.int32, (8, 768), 1)
     r128 = lax.broadcasted_iota(jnp.int32, (128, 768), 0)
@@ -460,12 +470,10 @@
     khop[1].wait_recv()
     for n, d in enumerate((0, 1, 7)):
         scores(d, n % 2)
-    z_wait(2)
-    z_start(3)
     scores(2, 1)
+    scores(6, 0)
     v_hop(0)
     v_start(1)
-    scores(6, 0)
     scores(3, 1)
     scores(5, 0)
     origin = [[lax.rem(y + r, 4) * 2 + (core if c == 0 else 1 - core) for r in range(4)] for c in range(2)]
@@ -477,7 +485,8 @@
 
     hspread.third(0)
     hspread.third(1)
-    z_wait(3)
+    z_wait(3, 0)
+    z_wait(3, 1)
     scores(4, 1)
     for h in range(2):
         hspread.arrived(h, 0, 3, 4, 6)
@@ -597,7 +606,7 @@
         c = add(acc[h], 1, h, ((1, 2),))
         s = slice(256 * h, 256 * h + 256)
         out[s, :] = (mixed[s, :] + gate[s, :] * c).astype(BF)
-    for group in (left, right, khop, *vleft, *vright, *vhop, up, down, *id_steps,
+    for group in (left, right, khop, *vleft, *vright, *vhop, *pieces.values(), *id_steps,
                   *sends[0], *sends[1], *(p for sp in (hspread, *spread) for p in sp.copies)):
         for c in group:
             c.wait_send()
@@ -632,7 +641,7 @@
             vm((2, 4, 4, 272, 128), BF), vm((2, 4, 4, 272, 128), BF), vm((2, 4, 2, 256, 128), BF),
             vm((2, rows, 128), BF), vm((2, 2, 4, 2, 256, 128), BF), vm((rows, 256), F32), vm((rows, 256), F32),
             dma((24,)), dma((2, 4)), dma((2, 4)), dma((2,)), dma((2,)), dma((2, 2, 2)), dma((2, 2, 2)),
-            dma((2, 2)), dma((2, 2)), dma((2, 4)), dma((2, 4)), dma((2, 4)), dma((2, 4)),
+            dma((2, 2)), dma((2, 2)), dma((2, 4, 2)), dma((2, 4, 2)), dma((2, 4)), dma((2, 4)),
             dma((2, 4, 4)), dma((2, 4, 4)), dma((3, 2, 7)), dma((3, 2, 7)),
         ],
         compiler_params=params(62, collective_id=0, has_side_effects=True),

time: 91.8 us -> 91.6 us (level)
  no operation moved by 1% of the time
where the time goes in v4:
time: 91.6 us; the launch traced here: 91.4 us
  Pallas kernels  89.8 us (98%)
  local copies, waits for them, and re-layouts  1.67 us (2%)
    pallas_call x1, Pallas kernels, local(): pl.pallas_call(layer_kernel, out_shape=sds((rows, 256), BF), in_specs=[AN...  89.8 us

profile of v4, /device:TPU:1, one launch (start us, length us, event | category | flops | bytes accessed | tf_op | source)
XLA Modules:
  0.0 91.4 jit_solution(9426626841029166387)
XLA Ops:
  0.0 89.8 %layer.1 = bf16[512,256]{1,0:T(8,128)(2,1)} custom-call(bf16[12,96,2048]{2,1,0:T(8,128)(2,1)} %store.1, bf16[2048,256]{1,0:T(8,128)(2,1)} %wk.1, bf16[2048,256]{1,0:T(8,128)(2,1)} %wv.1, bf16[512,2048]{1,0:T(8,128)(2,1)} %tok.1, bf16[2048,256]{1,0:T(8,128)(2,1)} %wq.1, bf16[2048,128]{1,0:T(8,128)(2,1)} %wg.1, bf16[2048,128]{1,0:T(8,128)(2,1)} %mq.1, ...), custom_call_target="tpu_custom_call" | custom-call | flops 30000001024 | bytes 4000000 | tf_op jit(solution)/shard_map/layer/pallas_call | solution.py:628
  89.8 1.7 %copy.23 = bf16[512,256]{1,0:T(8,128)(2,1)} copy(bf16[512,256]{1,0:T(8,128)(2,1)} %layer.1) | data formatting | bytes 524288

commit v5 on v4

--- a/solution.py
+++ b/solution.py
@@ -37,6 +37,12 @@
 
 def head_normed(y):
     return y * lax.rsqrt(jnp.mean(y * y, axis=-1, keepdims=True) + 1e-06)
+
+
+def dg3(a, b, ca, cb):
+    ah, bh = a.astype(BF), b.astype(BF)
+    al, bl = (a - ah.astype(F32)).astype(BF), (b - bh.astype(F32)).astype(BF)
+    return dg(ah, bh, ca, cb) + (dg(al, bh, ca, cb) + dg(ah, bl, ca, cb))
 
 
 def exact_sum_dot(left, x, ca, cb, swap):
@@ -82,7 +88,7 @@
     yield
     unit = k * lax.rsqrt(exact_sum_dot(ones, k * k, 1, 0, True) + 1e-06)
     rate_key = unit * rate
-    s_vs[...] = pltpu.roll(v, 64, 1).astype(BF)
+    s_vs[...] = pltpu.roll(v, 64, 1)
     for c in range(chunks):
         s = slice(64 * c, 64 * c + 64)
         f = log_fade[s]
@@ -92,10 +98,10 @@
         fo = jnp.exp(end - cumul)
         s_a[s, :] = -unit[s] * jnp.exp(cumul - f)
         s_q[s, :] = q[s] * jnp.exp(cumul)
-        s_ki[s, :] = (k[s] * ei).astype(BF)
-        s_ri[s, :] = (rate_key[s] * ei).astype(BF)
-        s_kf[s, :] = (k[s] * fo).astype(BF)
-        s_rf[s, :] = (rate_key[s] * fo).astype(BF)
+        s_ki[s, :] = k[s] * ei
+        s_ri[s, :] = rate_key[s] * ei
+        s_kf[s, :] = k[s] * fo
+        s_rf[s, :] = rate_key[s] * fo
         s_e[c:c + 1, :] = jnp.exp(end)
 
     yield
@@ -113,10 +119,10 @@
         cs = [slice(64 * c, 64 * c + 64) for c in range(g * group, (g + 1) * group)]
         G0, G1, PW, X, VL, VR = [], [], [], [], [], []
         for s in cs:
-            a, qq = s_a[s, :].astype(BF), s_q[s, :].astype(BF)
+            a, qq = s_a[s, :], s_q[s, :]
             ki, ri = s_ki[s, :], s_ri[s, :]
-            G0.append(dg(cat([only(a, left), only(qq, left)], 0), cat([ri, ki], 0), 1, 1))
-            G1.append(dg(cat([only(a, right), only(qq, right)], 0), cat([ki, ri], 0), 1, 1))
+            G0.append(dg3(cat([only(a, left), only(qq, left)], 0), cat([ri, ki], 0), 1, 1))
+            G1.append(dg3(cat([only(a, right), only(qq, right)], 0), cat([ki, ri], 0), 1, 1))
         for i, s in enumerate(cs):
             vs = s_vs[s, :]
             VR.append(only(vs, right))
@@ -124,38 +130,36 @@
             L = cat([only(G0[i][:64], sr), only(G1[i][:64], sl)], 0)
             PW.append(cat([only(G0[i][:64], sl), only(G1[i][:64], sr)], 0))
             a = s_a[s, :]
-            X.append(cat([only(a, left), only(a, right)], 0) + bdot(L, cat([VL[i], VR[i]], 0)))
+            X.append(cat([only(a, left), only(a, right)], 0) + dg3(L, cat([VL[i], VR[i]], 0), 1, 0))
         for it in range(6):
             for i in range(group):
-                p16 = PW[i].astype(BF)
                 if it < 5:
-                    px = dg(p16, cat([p16, X[i].astype(BF)], 1), 1, 0)
+                    px = dg3(PW[i], cat([PW[i], X[i]], 1), 1, 0)
                     PW[i] = px[:, :128]
                     X[i] = X[i] + px[:, 128:]
                 else:
-                    X[i] = X[i] + dg(p16, X[i].astype(BF), 1, 0)
+                    X[i] = X[i] + dg3(PW[i], X[i], 1, 0)
         MM, NN, PC, OO = [], [], [], []
         for i, s in enumerate(cs):
-            x16 = X[i].astype(BF)
+            x16 = X[i]
             h0 = cat([x16[:64], VR[i]], 0)
             h1 = cat([VL[i], x16[64:]], 0)
-            y0 = bdot(only(G0[i][64:], upto), h0)
-            y1 = bdot(only(G1[i][64:], upto), h1)
+            y0 = dg3(only(G0[i][64:], upto), h0, 1, 0)
+            y1 = dg3(only(G1[i][64:], upto), h1, 1, 0)
             qq = s_q[s, :]
-            PC.append(cat([only(y0 + qq, left), only(y1 + qq, right)], 0).astype(BF))
+            PC.append(cat([only(y0 + qq, left), only(y1 + qq, right)], 0))
             OO.append(only(y0, right) + only(y1, left))
             kf, rf = s_kf[s, :], s_rf[s, :]
             f = cat([only(rf, left), only(kf, left), only(kf, right), only(rf, right)], 0)
-            tr = dg(cat([h0, h1], 0), f, 0, 0)
+            tr = dg3(cat([h0, h1], 0), f, 0, 0)
             e = s_e[g * group + i:g * group + i + 1, :]
             zz = jnp.zeros((128, 128), F32)
-            MM.append((jnp.where(same, tr, zz) + jnp.where(eye, e, zz)).astype(BF))
+            MM.append(jnp.where(same, tr, zz) + jnp.where(eye, e, zz))
             NN.append(jnp.where(same, zz, tr))
         for i, s in enumerate(cs):
-            s16 = state.astype(BF)
-            o = dg(PC[i], s16, 1, 1)
+            o = dg3(PC[i], state, 1, 1)
             s_o[s, :] = OO[i] + o[:64] + o[64:]
-            state = dg(s16, MM[i], 1, 0) + NN[i]
+            state = dg3(state, MM[i], 1, 0) + NN[i]
         yield
     o = pltpu.roll(s_o[...], 64, 1)
     centred = o - exact_sum_dot(ones, o, 1, 0, True) * (1.0 / 64)
@@ -468,12 +472,12 @@
     right[3].wait_recv()
     khop[0].wait_recv()
     khop[1].wait_recv()
+    v_hop(0)
+    v_start(1)
     for n, d in enumerate((0, 1, 7)):
         scores(d, n % 2)
     scores(2, 1)
     scores(6, 0)
-    v_hop(0)
-    v_start(1)
     scores(3, 1)
     scores(5, 0)
     origin = [[lax.rem(y + r, 4) * 2 + (core if c == 0 else 1 - core) for r in range(4)] for c in range(2)]
@@ -554,6 +558,8 @@
         send(c, 2, 0)
         values(c, 5, 0)
         send(c, 3, 0)
+
+    def others(c):
         for n, d in enumerate((2, 6, 1, 7, 0)):
             values(c, d, (n + 1) % 2)
 
@@ -570,30 +576,34 @@
     v_wait(0)
     begin(0)
     v_hop(1)
+    others(0)
     step(0, 1)
-    step(0, 2)
     v_wait(1)
     begin(1)
+    step(0, 2)
+    others(1)
+    step(1, 1)
     step(0, 3)
-    step(1, 1)
+    step(1, 2)
     settle(0)
-    step(1, 2)
+    step(1, 3)
     spread[0].second(0)
     spread[0].second(1)
-    step(1, 3)
+    settle(1)
     spread[0].third(0)
     spread[0].third(1)
     acc = []
     for h in range(2):
-        a = dg(att[0, 256 * h:256 * h + 256, :], weight(wcv, 256, 0, 0, 0), 1, 0)
-        spread[0].arrived(h, 0, 3, 4, 6)
-        acc.append(add(a, 0, h, rest))
-    settle(1)
-    for h in range(2):
-        acc[h] = acc[h] + dg(att[1, 256 * h:256 * h + 256, :], weight(wcv, 256, 0, 0, 128), 1, 0)
+        s = slice(256 * h, 256 * h + 256)
+        a = dg(att[0, s, :], weight(wcv, 256, 0, 0, 0), 1, 0)
+        acc.append(a + dg(att[1, s, :], weight(wcv, 256, 0, 0, 128), 1, 0))
+        spread[0].arrived(h, 0, 3, 4)
+        acc[h] = add(acc[h], 0, h, rest[:-2] + rest[-1:])
     spread[1].second(0)
     spread[1].second(1)
     for h in range(2):
+        spread[0].arrived(h, 6)
+        acc[h] = add(acc[h], 0, h, rest[-2:-1])
         spread[1].arrived(h, 0)
         acc[h] = add(acc[h], 1, h, ((0, 3), (0, 1), (1, 0)))
     spread[1].third(0)
@@ -635,7 +645,7 @@
             w128(), w128(), vm(cross_out.shape, BF), vm(mix_out.shape, BF), vm(gate_up.shape, BF),
             vm((48, 96, 256), BF), vm((48, 96, 128), BF), vm((48, 96, 128), BF), vm((NZ, rows, 256), BF),
             vm((8, 8, 128), jnp.int32), vm((8, 128), jnp.int32), pltpu.SMEM((8, 128), jnp.int32), b(), b(),
-            f(), f(), b(), b(), b(), b(), b(), vm((8, 128), F32), f(),
+            f(), f(), f(), f(), f(), f(), f(), vm((8, 128), F32), f(),
             vm((2, 768, 256), BF), vm((2, 768, 128), BF), vm((NZ, rows, 768), BF),
             vm((2, NZ, rows, 128), F32), vm((64, 128), F32),
             vm((2, 4, 4, 272, 128), BF), vm((2, 4, 4, 272, 128), BF), vm((2, 4, 2, 256, 128), BF),

time: 91.6 us -> 89 us (0.972)
  Pallas kernels: 89.8 us -> 86.7 us
    pallas_call x1, Pallas kernels: 89.8 us -> 86.7 us  [local(): pl.pallas_call(layer_kernel, out_shape=sds((rows, 256), BF), in_specs=[AN...]
where the time goes in v5:
time: 89 us; the launch traced here: 88.4 us
  Pallas kernels  86.7 us (97%)
  local copies, waits for them, and re-layouts  1.67 us (2%)
    pallas_call x1, Pallas kernels, local(): pl.pallas_call(layer_kernel, out_shape=sds((rows, 256), BF), in_specs=[AN...  86.7 us

profile of v5, /device:TPU:1, one launch (start us, length us, event | category | flops | bytes accessed | tf_op | source)
XLA Modules:
  0.0 88.4 jit_solution(15996476338947351994)
XLA Ops:
  0.0 86.7 %layer.1 = bf16[512,256]{1,0:T(8,128)(2,1)} custom-call(bf16[12,96,2048]{2,1,0:T(8,128)(2,1)} %store.1, bf16[2048,256]{1,0:T(8,128)(2,1)} %wk.1, bf16[2048,256]{1,0:T(8,128)(2,1)} %wv.1, bf16[512,2048]{1,0:T(8,128)(2,1)} %tok.1, bf16[2048,256]{1,0:T(8,128)(2,1)} %wq.1, bf16[2048,128]{1,0:T(8,128)(2,1)} %wg.1, bf16[2048,128]{1,0:T(8,128)(2,1)} %mq.1, ...), custom_call_target="tpu_custom_call" | custom-call | flops 30000001024 | bytes 4000000 | tf_op jit(solution)/shard_map/layer/pallas_call | solution.py:638
  86.7 1.7 %copy.23 = bf16[512,256]{1,0:T(8,128)(2,1)} copy(bf16[512,256]{1,0:T(8,128)(2,1)} %layer.1) | data formatting | bytes 524288
